TPU v7x, 128 devices: a whole 4x4x4 slice. The times are simulated.
128 devices in a mesh: sp: 32 (over z, y, core), tp: 4 (over x).
Axes of the slice: x: 4, y: 4, z: 4, core: 2. Of those that a mesh axis runs over, the one named last changes fastest.
Arguments:
- tokens: bfloat16 [4096, 1024], P('sp', 'tp'), may hold values from -6 to 6
- norm_gain: float32 [1024], replicated, may hold values from 0.1 to 1.9
- attn_query: bfloat16 [1024, 512], P('sp', 'tp'), may hold values from -0.1875 to 0.1875
- attn_key: bfloat16 [1024, 256], P('sp', 'tp'), may hold values from -0.1875 to 0.1875
- attn_value: bfloat16 [1024, 256], P('sp', 'tp'), may hold values from -0.1875 to 0.1875
- sink_logit: float32 [8], P('tp'), may hold values from 2 to 7
- delta_query: bfloat16 [1024, 512], P('sp', 'tp'), may hold values from -0.1875 to 0.1875
- delta_key: bfloat16 [1024, 512], P('sp', 'tp'), may hold values from -0.1875 to 0.1875
- delta_value: bfloat16 [1024, 512], P('sp', 'tp'), may hold values from -0.1875 to 0.1875
- delta_gate: bfloat16 [1024, 512], P('sp', 'tp'), may hold values from -0.1875 to 0.1875
- beta_weight: bfloat16 [1024, 8, 2], P('sp', 'tp'), may hold values from -0.1875 to 0.1875
- decay_weight: bfloat16 [1024, 8, 2], P('sp', 'tp'), may hold values from -0.1875 to 0.1875
- beta_shift: float32 [2, 8], P(None, 'tp'), may hold values from -5 to -2
- decay_log: float32 [2, 8], P(None, 'tp'), may hold values from -2.5 to 1
- out_gain: float32 [64], replicated, may hold values from 0.1 to 1.9
- attn_out: bfloat16 [512, 1024], P('tp', 'sp'), may hold values from -1.5 to 1.5
- delta_out: bfloat16 [512, 1024], P('tp', 'sp'), may hold values from -0.25 to 0.25
Outputs:
- mixed: bfloat16 [4096, 1024], P(('sp', 'tp'))
All inputs are finite; a program needn't handle non-finite values.
Results may differ from a plain program's by a relative error of at most 0.0045.
Values may be sent and summed in bfloat16 or wider, within the bound.
A program may use at most 64 MiB of HBM per device.

v0:
```python
import functools

import jax
import jax.numpy as jnp
from jax import lax
from jax.experimental import pallas as pl
from jax.experimental.pallas import tpu as pltpu
from jax.sharding import PartitionSpec as P

HEAD_DIM = 64
WINDOW = 64
norm_eps = 1e-06
MESH = pl.DeviceIdType.MESH
F32 = jnp.float32
BF16 = jnp.bfloat16
SUM_DTYPE = jnp.bfloat16
PARTS = 3


def exact(a, b, dims=((1,), (0,))):
    return lax.dot_general(
        a, b, (dims, ((), ())), precision=lax.Precision.HIGHEST, preferred_element_type=F32
    )


def plain(a, b, dims=((1,), (0,))):
    return lax.dot_general(a, b, (dims, ((), ())), preferred_element_type=F32)


def split(x):
    high = x.astype(BF16)
    return high, (x - high.astype(F32)).astype(BF16)


def close(a, b, dims=((1,), (0,))):
    (ca,), (cb,) = dims
    left = jnp.concatenate([a[0], a[1], a[0]], axis=ca)
    right = jnp.concatenate([b[0], b[0], b[1]], axis=cb)
    return plain(left, right, dims)


def near(a, b, dims=((1,), (0,))):
    a, b = split(a), split(b)
    return plain(a[0], b[0], dims) + (plain(a[1], b[0], dims) + plain(a[0], b[1], dims))


def silu(x):
    return x * jax.nn.sigmoid(x)


def unit_rows(x):
    return x * lax.rsqrt(jnp.sum(x * x, axis=-1, keepdims=True) + norm_eps)


def copy_to(src, dst, send, recv, device):
    return pltpu.make_async_remote_copy(
        src_ref=src,
        dst_ref=dst,
        send_sem=send,
        recv_sem=recv,
        device_id=device,
        device_id_type=MESH,
    )


class Gather:
    def __init__(self, n, me, tp, buf, send, recv, parts):
        self.nh = n // 2
        self.me, self.tp = me, tp
        self.lo, self.hi = lax.rem(me, 2), lax.div(me, 2)
        self.buf, self.send, self.recv = buf, send, recv
        self.parts = parts
        self.size = buf.shape[2] // parts

    def copy(self, b, route, p):
        target = (self.me + 2, self.me - 2, self.hi * 2 + 1 - self.lo)[route]
        cols = pl.ds(p * self.size, self.size)
        return copy_to(
            self.buf.at[b, :, cols],
            self.buf.at[b, :, cols],
            self.send.at[route, b, p],
            self.recv.at[b, p],
            (target, self.tp),
        )

    def can(self, route):
        return self.hi < self.nh - 1 if route == 0 else self.hi > 0

    def first(self, act):
        for p in range(self.parts):
            for route in (0, 1):
                pl.when(self.can(route))(lambda p=p, route=route: act(self.copy(self.me, route, p)))
            act(self.copy(self.me, 2, p))

    def begin(self):
        self.first(lambda c: c.start())

    def sides(self, d):
        return ((0, self.hi - d, self.hi - d >= 0), (1, self.hi + d, self.hi + d < self.nh))

    def step(self, d, use=None):
        for p in range(self.parts):
            if d < self.nh:
                for route, there, ok in self.sides(d):

                    @pl.when(ok)
                    def _(route=route, there=there):
                        b = there * 2 + self.lo
                        self.copy(b, 2, p).wait_recv()
                        pl.when(self.can(route))(lambda: self.copy(b, route, p).start())
                        self.copy(b, 2, p).start()
                        if use is not None:
                            use(b, p)

            for i, (_, there, ok) in enumerate(self.sides(d - 1)):
                if d == 1 and i == 1:
                    continue

                @pl.when(ok)
                def _(there=there):
                    b = there * 2 + 1 - self.lo
                    self.copy(b, 2, p).wait_recv()
                    if use is not None:
                        use(b, p)

    def drain(self):
        self.first(lambda c: c.wait_send())
        for d in range(1, self.nh):
            for p in range(self.parts):
                for route, there, ok in self.sides(d):

                    @pl.when(ok)
                    def _(route=route, there=there):
                        b = there * 2 + self.lo
                        pl.when(self.can(route))(lambda: self.copy(b, route, p).wait_send())
                        self.copy(b, 2, p).wait_send()


def layer_kernel(
    n, nt, heads, kvs, dheads,
    tok, gain_in, aq, ak, av, dq, dk, dv, dz, ao, do, ab, par, og_in, out,
    gain, og, kvw, in_sem, tokbuf, normed, wbuf, obuf, abbuf, acc, kvbuf, st, stbuf, o_loc, r_mat, joined, part, rsbuf,
    tok_s, tok_r, w_s, w_r, o_s, o_r, ab_s, ab_r, kv_s, kv_r, st_s, st_r, rs_s, rs_r,
):
    me, t = lax.axis_index("sp"), lax.axis_index("tp")
    rows, width = tok.shape
    kb = aq.shape[0]
    hd = HEAD_DIM
    aw, kw, dw = heads * hd, kvs * hd, dheads * hd
    mine = [(tok, tokbuf.at[t])]
    at = 0
    for w in (aq, dq, dk, dv, dz):
        mine.append((w, wbuf.at[me, :, pl.ds(at, w.shape[1])]))
        at += w.shape[1]
    mine += [(ak, kvw.at[0]), (av, kvw.at[1]), (gain_in, gain), (og_in, og)]
    mine += [(ao, obuf.at[me, pl.ds(0, aw)]), (do, obuf.at[me, pl.ds(aw, dw)])]
    mine = [pltpu.make_async_copy(a, b, in_sem.at[i]) for i, (a, b) in enumerate(mine)]
    for c in mine:
        c.start()
    bar = pltpu.get_barrier_semaphore()
    for d in range(1, n):
        pl.semaphore_signal(bar, inc=1, device_id=(lax.rem(me + d, n), t), device_id_type=MESH)
    for d in range(1, nt):
        pl.semaphore_signal(bar, inc=1, device_id=(me, lax.rem(t + d, nt)), device_id_type=MESH)
    pl.semaphore_wait(bar, n - 1 + nt - 1)

    for c in mine:
        c.wait()
    wbuf[me, :, at:] = jnp.concatenate([kvw[0], kvw[1]], axis=1)
    tok_copies = [
        copy_to(tokbuf.at[t], tokbuf.at[t], tok_s.at[d - 1], tok_r.at[t], (me, lax.rem(t + d, nt)))
        for d in range(1, nt)
    ]
    for c in tok_copies:
        c.start()
    wg = Gather(n, me, t, wbuf, w_s, w_r, PARTS)
    ogather = Gather(n, me, t, obuf, o_s, o_r, 1)
    wg.begin()

    def ab_copy(d):
        p = lax.rem(me + d, n)
        return copy_to(ab, abbuf.at[me], ab_s.at[d], ab_r.at[me], (p, t))

    for d in range(1, n):
        ab_copy(d).start()
    abbuf[me] = ab[...]
    for d in range(1, nt):
        j = lax.rem(t + d, nt)
        copy_to(tokbuf.at[t], tokbuf.at[j], tok_s.at[d - 1], tok_r.at[j], (me, j)).wait_recv()
    total = jnp.zeros((rows, 1), F32)
    for j in range(nt):
        x = tokbuf[j].astype(F32)
        total += jnp.sum(x * x, axis=-1, keepdims=True)
    inverse = lax.rsqrt(total / (nt * width) + norm_eps)
    per = width // kb
    for j in range(nt):
        x = (tokbuf[j].astype(F32) * inverse * gain[:, j * width : (j + 1) * width]).astype(BF16)
        for i in range(per):
            normed[j * per + i] = x[:, i * kb : (i + 1) * kb]
    acc[...] = plain(normed[me], wbuf[me])

    half = wbuf.shape[2] // PARTS

    def use(b, p):
        cols = slice(p * half, (p + 1) * half)
        acc[:, cols] += plain(normed[b], wbuf[b, :, cols])

    for d in range(1, n // 2 + 1):
        wg.step(d, use)
    ogather.begin()

    kvbuf[WINDOW : WINDOW + rows] = acc[:, aw + 4 * dw :].astype(BF16)

    @pl.when(me == 0)
    def _():
        kvbuf[:WINDOW] = jnp.zeros((WINDOW, 2 * kw), BF16)

    @pl.when(me == n - 1)
    def _():
        kvbuf[WINDOW + rows :] = jnp.zeros((WINDOW, 2 * kw), BF16)

    base = aw
    for d in range(1, n):
        p = lax.rem(me + d, n)
        copy_to(ab, abbuf.at[p], ab_s.at[d], ab_r.at[p], (p, t)).wait_recv()
    tail = plain(abbuf[0], normed[0], ((1,), (1,)))
    for b in range(1, n):
        tail += plain(abbuf[b], normed[b], ((1,), (1,)))
    beta_t = jax.nn.sigmoid(tail + par[:, 0:1])
    soft = jnp.maximum(tail, 0.0) + jnp.log1p(jnp.exp(-jnp.abs(tail)))
    g_t = par[:, 1:2] * soft
    ri = lax.broadcasted_iota(jnp.int32, (rows, rows), 0)
    ci = lax.broadcasted_iota(jnp.int32, (rows, rows), 1)
    incl = (ri >= ci, ri <= ci)
    strict = (ri > ci, ri < ci)
    na = ab.shape[0]
    cum_t = [exact(g_t, jnp.where(m, 1.0, 0.0).astype(F32)) for m in (incl[1], incl[0])]
    stack = [beta_t] + cum_t
    if 3 * na < 128:
        stack.append(jnp.zeros((128 - 3 * na, rows), F32))
    columns = jnp.concatenate(stack, axis=0).T

    def head_to(p):
        up = copy_to(
            kvbuf.at[pl.ds(rows, WINDOW)], kvbuf.at[pl.ds(0, WINDOW)],
            kv_s.at[0], kv_r.at[0], (me + 1, t),
        )
        down = copy_to(
            kvbuf.at[pl.ds(WINDOW, WINDOW)], kvbuf.at[pl.ds(WINDOW + rows, WINDOW)],
            kv_s.at[1], kv_r.at[1], (me - 1, t),
        )
        return (up, down)[p]

    pl.when(me < n - 1)(lambda: head_to(0).start())
    pl.when(me > 0)(lambda: head_to(1).start())

    chains = []
    qs = []
    for h in range(dheads):
        def cols(i):
            lo_c = base + i * dw + h * hd
            return acc[:, lo_c : lo_c + hd].astype(BF16).astype(F32)

        q = unit_rows(silu(cols(0))) * hd ** (-0.5)
        k = unit_rows(silu(cols(1)))
        v = silu(cols(2))
        kk = near(k, k, ((1,), (1,)))
        qk = near(q, k, ((1,), (1,)))
        for r in range(2):
            c = h * 2 + r
            lane = 2 * dheads + c
            at = (1 + r) * na + lane
            gcol = columns[:, at : at + 1]
            grow = cum_t[r][lane : lane + 1, :]
            beta = columns[:, c : c + 1]
            decay = jnp.where(incl[r], jnp.exp(jnp.minimum(gcol - grow, 0.0)), 0.0)
            a = jnp.where(strict[r], beta * kk * decay, 0.0)
            eg = jnp.exp(gcol)
            last = gcol[rows - 1 : rows, :] if r == 0 else gcol[0:1, :]
            chains.append(
                dict(
                    r=r, h=h, a=a, rhs=jnp.concatenate([beta * v, beta * k * eg], axis=1),
                    pm=qk * decay, qe=q * eg, kd=(k * jnp.exp(last - gcol)).T, last=last,
                )
            )
    size = 1
    while (1 << size) <= rows:
        size += 1
    levels = size - 1
    eye = jnp.where(ri == ci, 1.0, 0.0).astype(F32)
    xor = ri ^ ci
    inv = [eye - jnp.where(xor == 1, ch["a"], 0.0) for ch in chains]
    pairs = [split(ch["a"]) for ch in chains]
    ogather.step(1)
    for lv in range(1, levels):
        m = jnp.where((xor >> lv) == 1, 1.0, 0.0).astype(BF16)
        xs = [split(x) for x in inv]
        left = [close(x, (m * a[0], m * a[1])) for x, a in zip(xs, pairs)]
        inv = [x - close(split(y), z) for x, y, z in zip(inv, left, xs)]
    sols = [split(close(split(x), split(ch["rhs"]))) for x, ch in zip(inv, chains)]
    outs = [close(split(ch["kd"]), s) for ch, s in zip(chains, sols)]
    e64 = jnp.where(
        lax.broadcasted_iota(jnp.int32, (hd, hd), 0)
        == lax.broadcasted_iota(jnp.int32, (hd, hd), 1), 1.0, 0.0,
    ).astype(F32)
    for ch, s in zip(chains, outs):
        full = jnp.concatenate([s[:, :hd], jnp.exp(ch["last"]) * e64 - s[:, hd:]], axis=1)
        st[ch["r"], ch["h"]] = full.astype(BF16)
    def state_copy(r, p):
        return copy_to(st.at[r], stbuf.at[me], st_s.at[p], st_r.at[me], (p, t))

    def state_all(act):
        for d in range(n - 1, 0, -1):
            pl.when(me + d < n)(lambda d=d: act(state_copy(0, me + d)))
            pl.when(me - d >= 0)(lambda d=d: act(state_copy(1, me - d)))

    state_all(lambda c: c.start())
    inner = [close(split(ch["pm"]), s) for ch, s in zip(chains, sols)]
    for ch, s in zip(chains, inner):
        o_loc[ch["r"], ch["h"]] = s[:, :hd]
        r_mat[ch["r"], ch["h"]] = ch["qe"] - s[:, hd:]


    ogather.step(2)

    pl.when(me > 0)(lambda: head_to(0).wait_recv())
    pl.when(me < n - 1)(lambda: head_to(1).wait_recv())
    span = rows + 2 * WINDOW
    qi = lax.broadcasted_iota(jnp.int32, (rows, span), 0)
    kj = lax.broadcasted_iota(jnp.int32, (rows, span), 1) - WINDOW
    pos = kj + me * rows
    allowed = (jnp.abs(qi - kj) <= WINDOW) & (pos >= 0) & (pos < n * rows)
    for h in range(heads):
        g = h // (heads // kvs)
        q = acc[:, h * hd : (h + 1) * hd].astype(BF16)
        s = plain(q, kvbuf[:, g * hd : (g + 1) * hd], ((1,), (1,))) * hd ** (-0.5)
        s = jnp.where(allowed, s, -jnp.inf)
        sink = par[h : h + 1, 2:3]
        m = jnp.maximum(jnp.max(s, axis=-1, keepdims=True), sink)
        e = jnp.exp(s - m)
        p = e / (jnp.sum(e, axis=-1, keepdims=True) + jnp.exp(sink - m))
        o = plain(p.astype(BF16), kvbuf[:, kw + g * hd : kw + (g + 1) * hd])
        joined[:, h * hd : (h + 1) * hd] = o.astype(BF16)
    for d in range(3, n // 2):
        ogather.step(d)

    for i in range(n):

        @pl.when(me != i)
        def _(i=i):
            copy_to(st.at[0], stbuf.at[i], st_s.at[i], st_r.at[i], (me, t)).wait_recv()

    fore = [jnp.zeros((hd, hd), F32)] * dheads
    back = [jnp.zeros((hd, hd), F32)] * dheads

    def enter(i, state, h, ok):
        both = jnp.where(ok, stbuf[i, h].astype(F32), ident)
        move, (high, low) = both[:, hd:].astype(BF16), split(state)
        return plain(move, high) + plain(move, low) + both[:, :hd]

    ident = jnp.concatenate([jnp.zeros((hd, hd), F32), e64], axis=1)
    for i in range(n - 1):
        fore = [enter(i, x, h, i < me) for h, x in enumerate(fore)]
        back = [enter(n - 1 - i, x, h, n - 1 - i > me) for h, x in enumerate(back)]
    if n // 2 > 2:
        ogather.step(n // 2)
    for h in range(dheads):
        o = o_loc[0, h] + o_loc[1, h] + near(r_mat[0, h], fore[h]) + near(r_mat[1, h], back[h])
        o = o * lax.rsqrt(jnp.mean(o * o, axis=-1, keepdims=True) + norm_eps) * og[...]
        lo_c = base + 3 * dw + h * hd
        gate = acc[:, lo_c : lo_c + hd].astype(BF16).astype(F32)
        joined[:, aw + h * hd : aw + (h + 1) * hd] = (o * silu(gate)).astype(BF16)

    cw = ao.shape[1]
    tr = rows // nt
    lhs = joined[...]
    for b in range(n):
        y = plain(lhs, obuf[b])
        for j in range(nt):
            part[j, :, b * cw : (b + 1) * cw] = y[j * tr : (j + 1) * tr].astype(SUM_DTYPE)
    rs_copies = [
        copy_to(
            part.at[lax.rem(t + d, nt)], rsbuf.at[d - 1], rs_s.at[d - 1], rs_r.at[d - 1],
            (me, lax.rem(t + d, nt)),
        )
        for d in range(1, nt)
    ]
    for c in rs_copies:
        c.start()
    for c in tok_copies:
        c.wait_send()
    for d in range(1, n):
        ab_copy(d).wait_send()
    wg.drain()
    ogather.drain()
    pl.when(me < n - 1)(lambda: head_to(0).wait_send())
    pl.when(me > 0)(lambda: head_to(1).wait_send())
    state_all(lambda c: c.wait_send())
    total = part[t].astype(F32)
    for d in range(1, nt):
        rs_copies[d - 1].wait_recv()
        total += rsbuf[d - 1].astype(F32)
    out[...] = total.astype(BF16)
    for c in rs_copies:
        c.wait_send()


def per_device(
    tokens, norm_gain, attn_query, attn_key, attn_value, sink_logit, delta_query, delta_key,
    delta_value, delta_gate, beta_weight, decay_weight, beta_shift, decay_log, out_gain,
    attn_out, delta_out,
):
    n, nt = lax.axis_size("sp"), lax.axis_size("tp")
    rows, width = tokens.shape
    kb = attn_query.shape[0]
    heads, kvs = attn_query.shape[1] // HEAD_DIM, attn_key.shape[1] // HEAD_DIM
    dheads = delta_query.shape[1] // HEAD_DIM
    ab = 2 * dheads
    wide = (2 * kvs + heads + 4 * dheads) * HEAD_DIM
    na = -(-2 * ab // 16) * 16
    gates = jnp.concatenate(
        [
            beta_weight.reshape(kb, ab).T, decay_weight.reshape(kb, ab).T,
            jnp.zeros((na - 2 * ab, kb), BF16),
        ],
        axis=0,
    )
    flat = lambda a, before: jnp.pad(a, (before, na - before - a.shape[0]))
    par = jnp.stack(
        [
            flat(beta_shift.T.reshape(ab), 0),
            flat(-jnp.exp(decay_log.T.reshape(ab)) / (rows * n), ab),
            flat(sink_logit, 0),
        ],
        axis=1,
    )
    cw = attn_out.shape[1]
    tr = rows // nt
    hd = HEAD_DIM
    kw = kvs * hd
    dma = pltpu.SemaphoreType.DMA
    vm = pl.BlockSpec(memory_space=pltpu.VMEM)
    hbm = pl.BlockSpec(memory_space=pl.ANY)
    return pl.pallas_call(
        functools.partial(layer_kernel, n, nt, heads, kvs, dheads),
        out_shape=jax.ShapeDtypeStruct((tr, n * cw), BF16),
        in_specs=[hbm] * 11 + [vm] * 2 + [hbm],
        out_specs=vm,
        scratch_shapes=[
            pltpu.VMEM((1, nt * width), F32),
            pltpu.VMEM((1, hd), F32),
            pltpu.VMEM((2, kb, kw), BF16),
            dma((12,)),
            pltpu.VMEM((nt, rows, width), BF16),
            pltpu.VMEM((n, rows, kb), BF16),
            pltpu.VMEM((n, kb, wide), BF16),
            pltpu.VMEM((n, (heads + dheads) * hd, cw), BF16),
            pltpu.VMEM((n, na, kb), BF16),
            pltpu.VMEM((rows, wide), F32),
            pltpu.VMEM((rows + 2 * WINDOW, 2 * kw), BF16),
            pltpu.VMEM((2, dheads, hd, 2 * hd), BF16),
            pltpu.VMEM((n, dheads, hd, 2 * hd), BF16),
            pltpu.VMEM((2, dheads, rows, hd), F32),
            pltpu.VMEM((2, dheads, rows, hd), F32),
            pltpu.VMEM((rows, (heads + dheads) * hd), BF16),
            pltpu.VMEM((nt, tr, n * cw), SUM_DTYPE),
            pltpu.VMEM((nt - 1, tr, n * cw), SUM_DTYPE),
            dma((nt - 1,)), dma((nt,)),
            dma((3, n, PARTS)), dma((n, PARTS)),
            dma((3, n, 1)), dma((n, 1)),
            dma((n,)), dma((n,)),
            dma((2,)), dma((2,)),
            dma((n,)), dma((n,)),
            dma((nt - 1,)), dma((nt - 1,)),
        ],
        compiler_params=pltpu.CompilerParams(
            collective_id=0, has_side_effects=True, vmem_limit_bytes=48 * 1024 * 1024
        ),
    )(
        tokens, norm_gain.reshape(1, nt * width), attn_query, attn_key, attn_value, delta_query,
        delta_key, delta_value, delta_gate, attn_out, delta_out, gates, par,
        out_gain.reshape(1, hd),
    )


def solution(mesh):
    return jax.shard_map(
        per_device,
        mesh=mesh,
        in_specs=(
            P("sp", "tp"), P(), P("sp", "tp"), P("sp", "tp"), P("sp", "tp"), P("tp"),
            P("sp", "tp"), P("sp", "tp"), P("sp", "tp"), P("sp", "tp"),
            P("sp", "tp", None), P("sp", "tp", None), P(None, "tp"), P(None, "tp"), P(),
            P("tp", "sp"), P("tp", "sp"),
        ),
        out_specs=P(("sp", "tp"), None),
        check_vma=False,
    )
```

profile of v0, /device:TPU:0, one launch (start us, length us, event | category | flops | bytes accessed | tf_op | source)
XLA Modules:
  0.0 141.9 jit_solution(2127549491843848398)
XLA Ops:
  0.0 0.0 copy-start.10
  0.0 0.0 copy-start.11
  0.0 0.0 copy-start.14
  0.0 0.0 copy-start.12
  0.0 0.0 copy-start.13
  0.0 0.0 copy-start
  0.0 0.1 pad.20.clone
  0.1 0.6 copy-done.10
  0.7 0.1 copy.25
  0.8 0.1 reshape.23
  0.9 0.0 copy-done.11
  0.9 0.1 copy.26
  1.0 0.1 div.9
  1.1 0.0 copy-done.14
  1.1 0.1 pad_bitcast_fusion
  1.1 0.0 copy-done.12
  1.1 0.0 copy-done.13
  1.2 0.1 maximum_maximum_fusion.ab
  1.2 0.1 copy.29.par
  1.3 0.0 copy-start.6
  1.3 0.0 copy-start.7
  1.3 0.0 copy-start.8
  1.3 0.0 copy-start.9
  1.3 0.9 copy.27.ao
  2.2 0.0 copy-start.1
  2.2 0.0 copy-start.2
  2.2 0.0 copy-start.3
  2.2 0.0 copy-start.4
  2.2 0.0 copy-start.5
  2.2 0.8 copy.28.do
  3.1 0.0 copy-done
  3.1 0.0 copy-done.6
  3.1 0.0 copy-done.7
  3.1 0.0 copy-done.8
  3.1 0.0 copy-done.9
  3.1 0.0 copy-done.1
  3.1 0.0 copy-done.2
  3.2 0.0 copy-done.3
  3.2 0.0 copy-done.4
  3.2 0.0 copy-done.5
  3.2 138.1 %shard_map.163 = bf16[32,1024]{1,0:T(8,128)(2,1)S(1)} custom-call(bf16[128,256]{1,0:T(8,128)(2,1)S(1)} %copy-done, f32[1,1024]{1,0:T(1,128)S(1)} %bitcast.17, bf16[32,128]{1,0:T(8,128)(2,1)S(1)} %copy-done.1, bf16[32,64]{1,0:T(8,128)(2,1)S(1)} %copy-done.2, bf16[32,64]{1,0:T(8,128)(2,1)S(1)} %copy-done.3, bf16[32,128]{1,0:T(8,128)(2,1)S(1)} %copy-done.4, ...), custom_call_target="tpu_custom_call" | custom-call | tf_op jit(solution)/shard_map/pallas_call | solution.py:444
  141.3 0.6 copy.31
  (4 shorter events, 0.0 us)
Async XLA Ops:
  0.0 0.7 copy-start.10
  0.0 0.9 copy-start.11
  0.0 1.1 copy-start.14
  0.0 1.1 copy-start.12
  0.0 1.1 copy-start.13
  0.0 3.1 %copy-start = (bf16[128,256]{1,0:T(8,128)(2,1)S(1)}, bf16[128,256]{1,0:T(8,128)(2,1)}, u32[]{:S(2)}) copy-start(bf16[128,256]{1,0:T(8,128)(2,1)} %tok.1) | copy-start | bytes 196612
  1.3 1.8 %copy-start.6 = (bf16[32,128]{1,0:T(8,128)(2,1)S(1)}, bf16[32,128]{1,0:T(8,128)(2,1)}, u32[]{:S(2)}) copy-start(bf16[32,128]{1,0:T(8,128)(2,1)} %dv.1) | copy-start | bytes 24580
  1.3 1.8 %copy-start.7 = (bf16[32,128]{1,0:T(8,128)(2,1)S(1)}, bf16[32,128]{1,0:T(8,128)(2,1)}, u32[]{:S(2)}) copy-start(bf16[32,128]{1,0:T(8,128)(2,1)} %dz.1) | copy-start | bytes 24580
  1.3 1.8 %copy-start.8 = (f32[1024]{0:T(1024)S(1)}, f32[1024]{0:T(1024)}, u32[]{:S(2)}) copy-start(f32[1024]{0:T(1024)} %param.18) | copy-start | bytes 12292
  1.3 1.8 %copy-start.9 = (f32[64]{0:T(128)S(1)}, f32[64]{0:T(128)}, u32[]{:S(2)}) copy-start(f32[64]{0:T(128)} %param.31) | copy-start | bytes 772
  2.2 0.9 copy-start.1
  2.2 0.9 copy-start.2
  2.2 0.9 copy-start.3
  2.2 0.9 copy-start.4
  2.2 0.9 copy-start.5
where the time goes:
time: 142 us
  Pallas kernels  138 us (97%)
  local copies, waits for them, and re-layouts  3.56 us (3%)
    pallas_call x1, Pallas kernels, per_device(): pl.pallas_call(functools.partial(layer_kernel, n, nt, heads, kvs, dheads)...  138 us
    unnamed x33, local copies, waits for them, and re-layouts  2.96 us

commit v1 on v0

v1 whole, which is shorter than its diff:
```python
import functools

import jax
import jax.numpy as jnp
from jax import lax
from jax.experimental import pallas as pl
from jax.experimental.pallas import tpu as pltpu
from jax.sharding import PartitionSpec as P

HEAD_DIM = 64
WINDOW = 64
norm_eps = 1e-06
MESH = pl.DeviceIdType.MESH
F32 = jnp.float32
BF16 = jnp.bfloat16
SUM_DTYPE = jnp.bfloat16


def exact(a, b, dims=((1,), (0,))):
    return lax.dot_general(
        a, b, (dims, ((), ())), precision=lax.Precision.HIGHEST, preferred_element_type=F32
    )


def plain(a, b, dims=((1,), (0,))):
    return lax.dot_general(a, b, (dims, ((), ())), preferred_element_type=F32)


def split(x):
    high = x.astype(BF16)
    return high, (x - high.astype(F32)).astype(BF16)


def close(a, b, dims=((1,), (0,))):
    (ca,), (cb,) = dims
    left = jnp.concatenate([a[0], a[1], a[0]], axis=ca)
    right = jnp.concatenate([b[0], b[0], b[1]], axis=cb)
    return plain(left, right, dims)


def near(a, b, dims=((1,), (0,))):
    a, b = split(a), split(b)
    return plain(a[0], b[0], dims) + (plain(a[1], b[0], dims) + plain(a[0], b[1], dims))


def silu(x):
    return x * jax.nn.sigmoid(x)


def unit_rows(x):
    return x * lax.rsqrt(jnp.sum(x * x, axis=-1, keepdims=True) + norm_eps)


def copy_to(src, dst, send, recv, device):
    return pltpu.make_async_remote_copy(
        src_ref=src,
        dst_ref=dst,
        send_sem=send,
        recv_sem=recv,
        device_id=device,
        device_id_type=MESH,
    )


RING = 4


def layer_kernel(
    n, nt, heads, kvs, dheads,
    tok, gain, aq, ak, av, dq, dk, dv, dz, ao, do, bw, gw, shift, dlog, sink_in, og, out,
    tokbuf, normed, wbuf, obuf, acc, kvbuf, st, stbuf, o_loc, r_mat, joined, part, rsbuf,
    tok_s, tok_r, w_s, w_r, o_s, o_r, kv_s, kv_r, st_s, st_r, rs_s, rs_r,
):
    me, t = lax.axis_index("sp"), lax.axis_index("tp")
    rows, width = tok.shape
    kb = aq.shape[0]
    hd = HEAD_DIM
    aw, kw, dw = heads * hd, kvs * hd, dheads * hd
    nb = 2 * dheads
    core, chip = lax.rem(me, 2), lax.div(me, 2)
    sa, sb = 1 + (RING - 1) * core, RING - (RING - 1) * core
    pa, pb = lax.rem(lax.div(chip, sa), RING), lax.rem(lax.div(chip, sb), RING)
    partner = me + 1 - 2 * core

    def at_pos(da, db):
        return 2 * (lax.rem(pa + da + RING, RING) * sa + lax.rem(pb + db + RING, RING) * sb) + core

    peers = [at_pos(1, 0), at_pos(-1, 0), at_pos(2, 0), at_pos(0, 1), at_pos(0, -1), at_pos(0, 2)]
    peers.append(partner)
    bar = pltpu.get_barrier_semaphore()
    for p in peers:
        pl.semaphore_signal(bar, inc=1, device_id=(p, t), device_id_type=MESH)
    for d in range(1, nt):
        pl.semaphore_signal(bar, inc=1, device_id=(me, lax.rem(t + d, nt)), device_id_type=MESH)

    mine = pl.ds(me * kb, kb)
    at = 0
    for w in (aq, dq, dk, dv, dz):
        wbuf[mine, at : at + w.shape[1]] = w[...]
        at += w.shape[1]
    wbuf[mine, at : at + 2 * kw] = jnp.concatenate([ak[...], av[...]], axis=1)
    at += 2 * kw
    goff = at
    gates = jnp.concatenate([bw[...], gw[...], gw[...]], axis=0).astype(F32)
    gates = jnp.concatenate([gates, jnp.zeros((128 - 3 * nb, kb), F32)], axis=0)
    gates = jnp.concatenate([gates, jnp.zeros((128, 128 - kb), F32)], axis=1)
    wbuf[mine, goff:] = gates.T[:kb].astype(BF16)
    obuf[mine, :aw] = ao[...]
    obuf[mine, aw:] = do[...]
    tokbuf[t] = tok[...]
    pl.semaphore_wait(bar, len(peers) + nt - 1)

    def w_copy(blk, k, device):
        ref = wbuf.at[pl.ds(blk * kb, kb)]
        return copy_to(ref, ref, w_s.at[k], w_r.at[blk], (device, t))

    sent = []

    def send(blk, k, device):
        c = w_copy(blk, k, device)
        c.start()
        sent.append(c)

    def landed(blk):
        w_copy(blk, 0, partner).wait_recv()

    hops = (0, 1, -1, 2)
    send(me, 0, at_pos(1, 0))
    send(me, 1, at_pos(-1, 0))
    send(me, 2, at_pos(2, 0))
    send(me, 3, at_pos(0, 1))
    send(me, 4, at_pos(0, -1))
    tok_copies = [
        copy_to(tok, tokbuf.at[t], tok_s.at[d - 1], tok_r.at[t], (me, lax.rem(t + d, nt)))
        for d in (1, 3, 2)
    ]
    for c in tok_copies:
        c.start()
    send(me, 15, partner)

    def share(blk, i, db):
        send(blk, 15 + i + RING * (db % RING), partner)

    def first(i):
        blk = at_pos(hops[i], 0)
        landed(blk)
        send(blk, 3 + 3 * i, at_pos(0, 1))
        send(blk, 4 + 3 * i, at_pos(0, -1))
        share(blk, i, 0)

    def second(i):
        for db in (1, -1):
            blk = at_pos(hops[i], db)
            landed(blk)
            if (db == -1) == (i in (0, 2)):
                send(blk, 5 + 3 * i, at_pos(0, -db))
            share(blk, i, db)

    def third(i):
        blk = at_pos(hops[i], 2)
        landed(blk)
        share(blk, i, 2)

    first(1)
    first(2)
    second(0)
    first(3)

    for d in range(1, nt):
        j = lax.rem(t + d, nt)
        copy_to(tok, tokbuf.at[j], tok_s.at[d - 1], tok_r.at[j], (me, j)).wait_recv()
    total = jnp.zeros((rows, 1), F32)
    for j in range(nt):
        x = tokbuf[j].astype(F32)
        total += jnp.sum(x * x, axis=-1, keepdims=True)
    inverse = lax.rsqrt(total / (nt * width) + norm_eps)
    for j in range(nt):
        cols = slice(j * width, (j + 1) * width)
        normed[:, cols] = (tokbuf[j].astype(F32) * inverse * gain[:, cols]).astype(BF16)

    second(1)
    second(2)
    third(0)
    second(3)
    third(1)
    third(2)
    third(3)
    for q in range(n // 2):
        landed(2 * q + 1 - core)

    acc[...] = plain(normed[...], wbuf[...])

    kvbuf[WINDOW : WINDOW + rows] = acc[:, aw + 4 * dw : goff].astype(BF16)

    @pl.when(me == 0)
    def _():
        kvbuf[:WINDOW] = jnp.zeros((WINDOW, 2 * kw), BF16)

    @pl.when(me == n - 1)
    def _():
        kvbuf[WINDOW + rows :] = jnp.zeros((WINDOW, 2 * kw), BF16)

    def head_to(p):
        up = copy_to(
            kvbuf.at[pl.ds(rows, WINDOW)], kvbuf.at[pl.ds(0, WINDOW)],
            kv_s.at[0], kv_r.at[0], (me + 1, t),
        )
        down = copy_to(
            kvbuf.at[pl.ds(WINDOW, WINDOW)], kvbuf.at[pl.ds(WINDOW + rows, WINDOW)],
            kv_s.at[1], kv_r.at[1], (me - 1, t),
        )
        return (up, down)[p]

    pl.when(me < n - 1)(lambda: head_to(0).start())
    pl.when(me > 0)(lambda: head_to(1).start())

    def o_copy(d, blk):
        ref = obuf.at[pl.ds(blk * kb, kb)]
        return copy_to(ref, ref, o_s.at[d], o_r.at[blk], (lax.rem(me + d, n), t))

    for d in range(1, n):
        o_copy(d, me).start()

    base = aw
    lane = lax.broadcasted_iota(jnp.int32, (1, 128), 1)
    shift_row = jnp.zeros((1, 128), F32)
    dlog_row = jnp.zeros((1, 128), F32)
    for h in range(dheads):
        for r in range(2):
            c = h * 2 + r
            shift_row = jnp.where(lane == c, shift[r, h], shift_row)
            dlog_row = jnp.where((lane == nb + c) | (lane == 2 * nb + c), dlog[r, h], dlog_row)
    coef = jnp.where((lane >= nb) & (lane < 3 * nb), -jnp.exp(dlog_row) / (rows * n), 0.0)
    tail = acc[:, goff:]
    soft = jnp.maximum(tail, 0.0) + jnp.log1p(jnp.exp(-jnp.abs(tail)))
    g = coef * soft
    ri = lax.broadcasted_iota(jnp.int32, (rows, rows), 0)
    ci = lax.broadcasted_iota(jnp.int32, (rows, rows), 1)
    incl = (ri >= ci, ri <= ci)
    strict = (ri > ci, ri < ci)
    cums = [exact(jnp.where(m, 1.0, 0.0).astype(F32), g) for m in incl]
    columns = jnp.where(
        lane < nb, jax.nn.sigmoid(tail + shift_row), jnp.where(lane < 2 * nb, cums[0], cums[1])
    )
    lines = columns.T

    chains = []
    for h in range(dheads):
        def cols(i):
            lo_c = base + i * dw + h * hd
            return acc[:, lo_c : lo_c + hd].astype(BF16).astype(F32)

        q = unit_rows(silu(cols(0))) * hd ** (-0.5)
        k = unit_rows(silu(cols(1)))
        v = silu(cols(2))
        kk = near(k, k, ((1,), (1,)))
        qk = near(q, k, ((1,), (1,)))
        for r in range(2):
            c = h * 2 + r
            at = (1 + r) * nb + c
            gcol = columns[:, at : at + 1]
            grow = lines[at : at + 1, :]
            beta = columns[:, c : c + 1]
            decay = jnp.where(incl[r], jnp.exp(jnp.minimum(gcol - grow, 0.0)), 0.0)
            a = jnp.where(strict[r], beta * kk * decay, 0.0)
            eg = jnp.exp(gcol)
            last = gcol[rows - 1 : rows, :] if r == 0 else gcol[0:1, :]
            chains.append(
                dict(
                    r=r, h=h, a=a, rhs=jnp.concatenate([beta * v, beta * k * eg], axis=1),
                    pm=qk * decay, qe=q * eg, kd=(k * jnp.exp(last - gcol)).T, last=last,
                )
            )
    size = 1
    while (1 << size) <= rows:
        size += 1
    levels = size - 1
    eye = jnp.where(ri == ci, 1.0, 0.0).astype(F32)
    xor = ri ^ ci
    inv = [eye - jnp.where(xor == 1, ch["a"], 0.0) for ch in chains]
    pairs = [split(ch["a"]) for ch in chains]
    for lv in range(1, levels):
        m = jnp.where((xor >> lv) == 1, 1.0, 0.0).astype(BF16)
        xs = [split(x) for x in inv]
        left = [close(x, (m * a[0], m * a[1])) for x, a in zip(xs, pairs)]
        inv = [x - close(split(y), z) for x, y, z in zip(inv, left, xs)]
    sols = [split(close(split(x), split(ch["rhs"]))) for x, ch in zip(inv, chains)]
    outs = [close(split(ch["kd"]), s) for ch, s in zip(chains, sols)]
    e64 = jnp.where(
        lax.broadcasted_iota(jnp.int32, (hd, hd), 0)
        == lax.broadcasted_iota(jnp.int32, (hd, hd), 1), 1.0, 0.0,
    ).astype(F32)
    for ch, s in zip(chains, outs):
        full = jnp.concatenate([s[:, :hd], jnp.exp(ch["last"]) * e64 - s[:, hd:]], axis=1)
        st[ch["r"], ch["h"]] = full.astype(BF16)
    def state_copy(r, p):
        return copy_to(st.at[r], stbuf.at[me], st_s.at[p], st_r.at[me], (p, t))

    def state_all(act):
        for d in range(n - 1, 0, -1):
            pl.when(me + d < n)(lambda d=d: act(state_copy(0, me + d)))
            pl.when(me - d >= 0)(lambda d=d: act(state_copy(1, me - d)))

    state_all(lambda c: c.start())
    inner = [close(split(ch["pm"]), s) for ch, s in zip(chains, sols)]
    for ch, s in zip(chains, inner):
        o_loc[ch["r"], ch["h"]] = s[:, :hd]
        r_mat[ch["r"], ch["h"]] = ch["qe"] - s[:, hd:]


    pl.when(me > 0)(lambda: head_to(0).wait_recv())
    pl.when(me < n - 1)(lambda: head_to(1).wait_recv())
    span = rows + 2 * WINDOW
    qi = lax.broadcasted_iota(jnp.int32, (rows, span), 0)
    kj = lax.broadcasted_iota(jnp.int32, (rows, span), 1) - WINDOW
    pos = kj + me * rows
    allowed = (jnp.abs(qi - kj) <= WINDOW) & (pos >= 0) & (pos < n * rows)
    for h in range(heads):
        g = h // (heads // kvs)
        q = acc[:, h * hd : (h + 1) * hd].astype(BF16)
        s = plain(q, kvbuf[:, g * hd : (g + 1) * hd], ((1,), (1,))) * hd ** (-0.5)
        s = jnp.where(allowed, s, -jnp.inf)
        sink = sink_in[h]
        m = jnp.maximum(jnp.max(s, axis=-1, keepdims=True), sink)
        e = jnp.exp(s - m)
        p = e / (jnp.sum(e, axis=-1, keepdims=True) + jnp.exp(sink - m))
        o = plain(p.astype(BF16), kvbuf[:, kw + g * hd : kw + (g + 1) * hd])
        joined[:, h * hd : (h + 1) * hd] = o.astype(BF16)

    for i in range(n):

        @pl.when(me != i)
        def _(i=i):
            copy_to(st.at[0], stbuf.at[i], st_s.at[i], st_r.at[i], (me, t)).wait_recv()

    fore = [jnp.zeros((hd, hd), F32)] * dheads
    back = [jnp.zeros((hd, hd), F32)] * dheads

    def enter(i, state, h, ok):
        both = jnp.where(ok, stbuf[i, h].astype(F32), ident)
        move, (high, low) = both[:, hd:].astype(BF16), split(state)
        return plain(move, high) + plain(move, low) + both[:, :hd]

    ident = jnp.concatenate([jnp.zeros((hd, hd), F32), e64], axis=1)
    for i in range(n - 1):
        fore = [enter(i, x, h, i < me) for h, x in enumerate(fore)]
        back = [enter(n - 1 - i, x, h, n - 1 - i > me) for h, x in enumerate(back)]
    for h in range(dheads):
        o = o_loc[0, h] + o_loc[1, h] + near(r_mat[0, h], fore[h]) + near(r_mat[1, h], back[h])
        o = o * lax.rsqrt(jnp.mean(o * o, axis=-1, keepdims=True) + norm_eps) * og[...]
        lo_c = base + 3 * dw + h * hd
        gate = acc[:, lo_c : lo_c + hd].astype(BF16).astype(F32)
        joined[:, aw + h * hd : aw + (h + 1) * hd] = (o * silu(gate)).astype(BF16)

    for d in range(1, n):
        o_copy(d, lax.rem(me + d, n)).wait_recv()
    tr = rows // nt
    y = plain(joined[...], obuf[...], ((1,), (1,)))
    for j in range(nt):
        part[j] = y[j * tr : (j + 1) * tr].astype(SUM_DTYPE)
    rs_copies = [
        copy_to(
            part.at[lax.rem(t + d, nt)], rsbuf.at[d - 1], rs_s.at[d - 1], rs_r.at[d - 1],
            (me, lax.rem(t + d, nt)),
        )
        for d in range(1, nt)
    ]
    for c in rs_copies:
        c.start()
    for c in tok_copies:
        c.wait_send()
    for c in sent:
        c.wait_send()
    for d in range(1, n):
        o_copy(d, me).wait_send()
    pl.when(me < n - 1)(lambda: head_to(0).wait_send())
    pl.when(me > 0)(lambda: head_to(1).wait_send())
    state_all(lambda c: c.wait_send())
    total = part[t].astype(F32)
    for d in range(1, nt):
        rs_copies[d - 1].wait_recv()
        total += rsbuf[d - 1].astype(F32)
    out[...] = total.astype(BF16)
    for c in rs_copies:
        c.wait_send()


def per_device(
    tokens, norm_gain, attn_query, attn_key, attn_value, sink_logit, delta_query, delta_key,
    delta_value, delta_gate, beta_weight, decay_weight, beta_shift, decay_log, out_gain,
    attn_out, delta_out,
):
    n, nt = lax.axis_size("sp"), lax.axis_size("tp")
    rows, width = tokens.shape
    kb = attn_query.shape[0]
    hd = HEAD_DIM
    heads, kvs = attn_query.shape[1] // hd, attn_key.shape[1] // hd
    dheads = delta_query.shape[1] // hd
    nb = 2 * dheads
    wide = (2 * kvs + heads + 4 * dheads) * hd + 128
    both = (heads + dheads) * hd
    cw = attn_out.shape[1]
    tr = rows // nt
    kw = kvs * hd
    assert n == 2 * RING * RING and cw == kb
    gates = lambda w: jnp.transpose(w, (1, 2, 0)).reshape(nb, kb)
    dma = pltpu.SemaphoreType.DMA
    vm = pl.BlockSpec(memory_space=pltpu.VMEM)
    sm = pl.BlockSpec(memory_space=pltpu.SMEM)
    return pl.pallas_call(
        functools.partial(layer_kernel, n, nt, heads, kvs, dheads),
        out_shape=jax.ShapeDtypeStruct((tr, n * cw), BF16),
        in_specs=[vm] * 13 + [sm] * 3 + [vm],
        out_specs=vm,
        scratch_shapes=[
            pltpu.VMEM((nt, rows, width), BF16),
            pltpu.VMEM((rows, nt * width), BF16),
            pltpu.VMEM((n * kb, wide), BF16),
            pltpu.VMEM((n * cw, both), BF16),
            pltpu.VMEM((rows, wide), F32),
            pltpu.VMEM((rows + 2 * WINDOW, 2 * kw), BF16),
            pltpu.VMEM((2, dheads, hd, 2 * hd), BF16),
            pltpu.VMEM((n, dheads, hd, 2 * hd), BF16),
            pltpu.VMEM((2, dheads, rows, hd), F32),
            pltpu.VMEM((2, dheads, rows, hd), F32),
            pltpu.VMEM((rows, both), BF16),
            pltpu.VMEM((nt, tr, n * cw), SUM_DTYPE),
            pltpu.VMEM((nt - 1, tr, n * cw), SUM_DTYPE),
            dma((nt - 1,)), dma((nt,)),
            dma((n - 1,)), dma((n,)),
            dma((n,)), dma((n,)),
            dma((2,)), dma((2,)),
            dma((n,)), dma((n,)),
            dma((nt - 1,)), dma((nt - 1,)),
        ],
        compiler_params=pltpu.CompilerParams(
            collective_id=0, has_side_effects=True, vmem_limit_bytes=48 * 1024 * 1024
        ),
    )(
        tokens, norm_gain.reshape(1, nt * width), attn_query, attn_key, attn_value, delta_query,
        delta_key, delta_value, delta_gate, attn_out.T, delta_out.T, gates(beta_weight),
        gates(decay_weight), beta_shift, decay_log, sink_logit, out_gain.reshape(1, hd),
    )


def solution(mesh):
    return jax.shard_map(
        per_device,
        mesh=mesh,
        in_specs=(
            P("sp", "tp"), P(), P("sp", "tp"), P("sp", "tp"), P("sp", "tp"), P("tp"),
            P("sp", "tp"), P("sp", "tp"), P("sp", "tp"), P("sp", "tp"),
            P("sp", "tp", None), P("sp", "tp", None), P(None, "tp"), P(None, "tp"), P(),
            P("tp", "sp"), P("tp", "sp"),
        ),
        out_specs=P(("sp", "tp"), None),
        check_vma=False,
    )
```

time: 142 us -> 69.5 us (0.49)
  the two profiles are of different devices: /device:TPU:0 before, /device:TPU:1 now
where the time goes in v1:
time: 69.5 us; the launch traced here: 68.8 us
  Pallas kernels  58.3 us (84%)
  local copies, waits for them, and re-layouts  10.4 us (15%)
    pallas_call x1, Pallas kernels, per_device(): pl.pallas_call(functools.partial(layer_kernel, n, nt, heads, kvs, dheads)...  58.3 us
    unnamed x35, local copies, waits for them, and re-layouts  10.4 us

profile of v1, /device:TPU:1, one launch (start us, length us, event | category | flops | bytes accessed | tf_op | source)
XLA Modules:
  0.0 68.8 jit_solution(3467760033383819800)
XLA Ops:
  0.0 0.0 copy-start.1
  0.0 0.0 copy-start.12
  0.0 0.0 copy-start.13
  0.0 0.0 copy-start.11
  0.0 0.7 copy-done.1
  0.7 0.0 copy-done.12
  0.7 0.0 copy-done.13
  0.7 0.0 copy-done.11
  0.7 0.0 copy-start
  0.7 0.8 %copy-done = bf16[128,256]{1,0:T(8,128)(2,1)S(1)} copy-done((bf16[128,256]{1,0:T(8,128)(2,1)S(1)}, bf16[128,256]{1,0:T(8,128)(2,1)}, u32[]{:S(2)}) %copy-start) | copy-done | bytes 65560
  1.6 0.0 copy-start.2
  1.6 0.7 %copy-done.2 = bf16[32,64]{1,0:T(8,128)(2,1)S(1)} copy-done((bf16[32,64]{1,0:T(8,128)(2,1)S(1)}, bf16[32,64]{1,0:T(8,128)(2,1)}, u32[]{:S(2)}) %copy-start.2) | copy-done | bytes 4120
  2.3 0.0 copy-start.3
  2.3 0.7 %copy-done.3 = bf16[32,64]{1,0:T(8,128)(2,1)S(1)} copy-done((bf16[32,64]{1,0:T(8,128)(2,1)S(1)}, bf16[32,64]{1,0:T(8,128)(2,1)}, u32[]{:S(2)}) %copy-start.3) | copy-done | bytes 4120
  3.0 0.0 copy-start.4
  3.0 0.7 %copy-done.4 = bf16[32,128]{1,0:T(8,128)(2,1)S(1)} copy-done((bf16[32,128]{1,0:T(8,128)(2,1)S(1)}, bf16[32,128]{1,0:T(8,128)(2,1)}, u32[]{:S(2)}) %copy-start.4) | copy-done | bytes 8216
  3.7 0.0 copy-start.5
  3.7 0.7 %copy-done.5 = bf16[32,128]{1,0:T(8,128)(2,1)S(1)} copy-done((bf16[32,128]{1,0:T(8,128)(2,1)S(1)}, bf16[32,128]{1,0:T(8,128)(2,1)}, u32[]{:S(2)}) %copy-start.5) | copy-done | bytes 8216
  4.4 0.0 copy-start.6
  4.4 0.7 %copy-done.6 = bf16[32,128]{1,0:T(8,128)(2,1)S(1)} copy-done((bf16[32,128]{1,0:T(8,128)(2,1)S(1)}, bf16[32,128]{1,0:T(8,128)(2,1)}, u32[]{:S(2)}) %copy-start.6) | copy-done | bytes 8216
  5.1 0.0 copy-start.7
  5.1 0.7 %copy-done.7 = bf16[32,128]{1,0:T(8,128)(2,1)S(1)} copy-done((bf16[32,128]{1,0:T(8,128)(2,1)S(1)}, bf16[32,128]{1,0:T(8,128)(2,1)}, u32[]{:S(2)}) %copy-start.7) | copy-done | bytes 8216
  5.8 0.0 copy-start.8
  5.8 0.7 %copy-done.8 = bf16[128,32]{0,1:T(8,128)(2,1)S(1)} copy-done((bf16[128,32]{0,1:T(8,128)(2,1)S(1)}, bf16[128,32]{0,1:T(8,128)(2,1)}, u32[]{:S(2)}) %copy-start.8) | copy-done | bytes 8216
  6.4 0.0 copy-start.9
  6.5 0.7 %copy-done.9 = bf16[128,32]{0,1:T(8,128)(2,1)S(1)} copy-done((bf16[128,32]{0,1:T(8,128)(2,1)S(1)}, bf16[128,32]{0,1:T(8,128)(2,1)}, u32[]{:S(2)}) %copy-start.9) | copy-done | bytes 8216
  7.1 0.0 copy-start.10
  7.1 0.7 copy-done.10
  7.8 0.0 copy-start.14
  7.8 0.7 copy-done.14
  8.5 0.0 copy-start.15
  8.5 0.7 copy-done.15
  9.2 0.0 copy-start.16
  9.2 0.7 copy-done.16
  9.8 58.3 %shard_map.163 = bf16[32,1024]{1,0:T(8,128)(2,1)S(1)} custom-call(bf16[128,256]{1,0:T(8,128)(2,1)S(1)} %copy-done, f32[1,1024]{1,0:T(1,128)S(1)} %bitcast.12, bf16[32,128]{1,0:T(8,128)(2,1)S(1)} %copy-done.1, bf16[32,64]{1,0:T(8,128)(2,1)S(1)} %copy-done.2, bf16[32,64]{1,0:T(8,128)(2,1)S(1)} %copy-done.3, bf16[32,128]{1,0:T(8,128)(2,1)S(1)} %copy-done.4, ...), custom_call_target="tpu_custom_call" | custom-call | tf_op jit(solution)/shard_map/pallas_call | solution.py:410
  68.2 0.6 copy.19
Async XLA Ops:
  0.0 0.7 %copy-start.1 = (bf16[32,128]{1,0:T(8,128)(2,1)S(1)}, bf16[32,128]{1,0:T(8,128)(2,1)}, u32[]{:S(2)}) copy-start(bf16[32,128]{1,0:T(8,128)(2,1)} %aq.1) | copy-start | bytes 24580
  0.0 0.7 %copy-start.12 = (bf16[32,2,2]{0,2,1:T(2,128)(2,1)S(1)}, bf16[32,2,2]{0,2,1:T(2,128)(2,1)}, u32[]{:S(2)}) copy-start(bf16[32,2,2]{0,2,1:T(2,128)(2,1)} %param.28) | copy-start | bytes 772
  0.0 0.7 %copy-start.13 = (f32[2,2]{1,0:T(2,128)S(1)}, f32[2,2]{1,0:T(2,128)}, u32[]{:S(2)}) copy-start(f32[2,2]{1,0:T(2,128)} %shift.1) | copy-start | bytes 52
  0.0 0.7 %copy-start.11 = (bf16[32,2,2]{0,2,1:T(2,128)(2,1)S(1)}, bf16[32,2,2]{0,2,1:T(2,128)(2,1)}, u32[]{:S(2)}) copy-start(bf16[32,2,2]{0,2,1:T(2,128)(2,1)} %param.27) | copy-start | bytes 772
  0.7 0.8 %copy-start = (bf16[128,256]{1,0:T(8,128)(2,1)S(1)}, bf16[128,256]{1,0:T(8,128)(2,1)}, u32[]{:S(2)}) copy-start(bf16[128,256]{1,0:T(8,128)(2,1)} %tok.1) | copy-start | bytes 196612
  1.6 0.7 %copy-start.2 = (bf16[32,64]{1,0:T(8,128)(2,1)S(1)}, bf16[32,64]{1,0:T(8,128)(2,1)}, u32[]{:S(2)}) copy-start(bf16[32,64]{1,0:T(8,128)(2,1)} %ak.1) | copy-start | bytes 12292
  2.3 0.7 %copy-start.3 = (bf16[32,64]{1,0:T(8,128)(2,1)S(1)}, bf16[32,64]{1,0:T(8,128)(2,1)}, u32[]{:S(2)}) copy-start(bf16[32,64]{1,0:T(8,128)(2,1)} %av.1) | copy-start | bytes 12292
  3.0 0.7 %copy-start.4 = (bf16[32,128]{1,0:T(8,128)(2,1)S(1)}, bf16[32,128]{1,0:T(8,128)(2,1)}, u32[]{:S(2)}) copy-start(bf16[32,128]{1,0:T(8,128)(2,1)} %dq.1) | copy-start | bytes 24580
  3.7 0.7 %copy-start.5 = (bf16[32,128]{1,0:T(8,128)(2,1)S(1)}, bf16[32,128]{1,0:T(8,128)(2,1)}, u32[]{:S(2)}) copy-start(bf16[32,128]{1,0:T(8,128)(2,1)} %dk.1) | copy-start | bytes 24580
  4.4 0.7 %copy-start.6 = (bf16[32,128]{1,0:T(8,128)(2,1)S(1)}, bf16[32,128]{1,0:T(8,128)(2,1)}, u32[]{:S(2)}) copy-start(bf16[32,128]{1,0:T(8,128)(2,1)} %dv.1) | copy-start | bytes 24580
  5.1 0.7 %copy-start.7 = (bf16[32,128]{1,0:T(8,128)(2,1)S(1)}, bf16[32,128]{1,0:T(8,128)(2,1)}, u32[]{:S(2)}) copy-start(bf16[32,128]{1,0:T(8,128)(2,1)} %dz.1) | copy-start | bytes 24580
  5.8 0.7 %copy-start.8 = (bf16[128,32]{0,1:T(8,128)(2,1)S(1)}, bf16[128,32]{0,1:T(8,128)(2,1)}, u32[]{:S(2)}) copy-start(bf16[128,32]{0,1:T(8,128)(2,1)} %param.32) | copy-start | bytes 24580
  6.4 0.7 %copy-start.9 = (bf16[128,32]{0,1:T(8,128)(2,1)S(1)}, bf16[128,32]{0,1:T(8,128)(2,1)}, u32[]{:S(2)}) copy-start(bf16[128,32]{0,1:T(8,128)(2,1)} %param.33) | copy-start | bytes 24580
  7.1 0.7 copy-start.10
  7.8 0.7 copy-start.14
  8.5 0.7 copy-start.15
  9.2 0.7 copy-start.16

commit v2 on v1

v2 whole, which is shorter than its diff:
```python
import functools

import jax
import jax.numpy as jnp
from jax import lax
from jax.experimental import pallas as pl
from jax.experimental.pallas import tpu as pltpu
from jax.sharding import PartitionSpec as P

HEAD_DIM = 64
WINDOW = 64
norm_eps = 1e-06
MESH = pl.DeviceIdType.MESH
F32 = jnp.float32
BF16 = jnp.bfloat16
SUM_DTYPE = jnp.bfloat16
RING = 4


def exact(a, b, dims=((1,), (0,))):
    return lax.dot_general(
        a, b, (dims, ((), ())), precision=lax.Precision.HIGHEST, preferred_element_type=F32
    )


def plain(a, b, dims=((1,), (0,))):
    return lax.dot_general(a, b, (dims, ((), ())), preferred_element_type=F32)


def split(x):
    high = x.astype(BF16)
    return high, (x - high.astype(F32)).astype(BF16)


def close(a, b, dims=((1,), (0,))):
    (ca,), (cb,) = dims
    left = jnp.concatenate([a[0], a[1], a[0]], axis=ca)
    right = jnp.concatenate([b[0], b[0], b[1]], axis=cb)
    return plain(left, right, dims)


def near(a, b, dims=((1,), (0,))):
    a, b = split(a), split(b)
    return plain(a[0], b[0], dims) + (plain(a[1], b[0], dims) + plain(a[0], b[1], dims))


def silu(x):
    return x * jax.nn.sigmoid(x)


def unit_rows(x):
    return x * lax.rsqrt(jnp.sum(x * x, axis=-1, keepdims=True) + norm_eps)


def copy_to(src, dst, send, recv, device):
    return pltpu.make_async_remote_copy(
        src_ref=src,
        dst_ref=dst,
        send_sem=send,
        recv_sem=recv,
        device_id=device,
        device_id_type=MESH,
    )


class Spread:
    def __init__(self, kb, core, z, y, t, buf, own, send_sem, recv_sem):
        self.kb, self.core, self.z, self.y, self.t = kb, core, z, y, t
        self.buf, self.own, self.send_sem, self.recv_sem = buf, own, send_sem, recv_sem
        self.started = []

    def chip(self, axis, da, db):
        dz, dy = (db, da) if axis == 0 else (da, db)
        return lax.rem(self.z + dz + RING, RING) * RING + lax.rem(self.y + dy + RING, RING)

    def send(self, src, blk, device):
        k = len(self.started)
        dst = self.buf.at[pl.ds(blk * self.kb, self.kb)]
        c = copy_to(src, dst, self.send_sem.at[k], self.recv_sem.at[blk], (device, self.t))
        c.start()
        self.started.append(c)

    def landed(self, blk):
        ref = self.buf.at[pl.ds(blk * self.kb, self.kb)]
        partner = 2 * (self.z * RING + self.y) + 1 - self.core
        copy_to(ref, ref, self.send_sem.at[0], self.recv_sem.at[blk], (partner, self.t)).wait_recv()

    def begin(self):
        me = 2 * self.chip(0, 0, 0) + self.core
        for da in (2, 1, -1):
            for axis in (0, 1):
                to = self.chip(axis, da, 0)
                for c in range(2):
                    self.send(self.own(c), me, 2 * to + c)
        self.send(self.own(1 - self.core), me, me + 1 - 2 * self.core)

    def forward(self):
        for r in (1, -1, 2):
            for axis in (0, 1):
                blk = 2 * self.chip(axis, r, 0) + axis
                self.landed(blk)
                for db in (2, 1, -1):
                    src = self.buf.at[pl.ds(blk * self.kb, self.kb)]
                    self.send(src, blk, 2 * self.chip(axis, 0, db) + self.core)

    def finish(self):
        self.landed(2 * self.chip(0, 0, 0) + 1 - self.core)
        for axis in (0, 1):
            for r in (0, 1, -1, 2):
                for db in (1, -1, 2):
                    self.landed(2 * self.chip(axis, r, db) + axis)

    def drain(self):
        for c in self.started:
            c.wait_send()


def layer_kernel(
    n, nt,
    tok_in, gain_in, aq_in, ak_in, av_in, dq_in, dk_in, dv_in, dz_in, ao_in, do_in, bw_in, gw_in,
    shift_in, dlog_in, sink_src, og_in, out,
    gain, wide_in, slim_in, oin, bw, gw, shift, dlog, sink_in, og, in_sem,
    tokbuf, normed, pack, wbuf, obuf, acc, kvbuf, st, stbuf, o_loc, r_mat, heads, other, part, rsbuf,
    tok_s, tok_r, w_s, w_r, o_s, o_r, kv_s, kv_r, st_s, st_r, h_s, h_r, rs_s, rs_r,
):
    me, t = lax.axis_index("sp"), lax.axis_index("tp")
    rows, width = tok_in.shape
    kb = aq_in.shape[0]
    hd = HEAD_DIM
    chips = n // 2
    core, chip = lax.rem(me, 2), lax.div(me, 2)
    z, y = lax.div(chip, RING), lax.rem(chip, RING)
    partner = me + 1 - 2 * core
    mine = pl.ds(me * kb, kb)

    loads = [
        (bw_in, bw), (gw_in, gw), (ak_in, slim_in.at[0]), (av_in, slim_in.at[1]),
        (aq_in, wide_in.at[0]), (dq_in, wide_in.at[1]), (dk_in, wide_in.at[2]),
        (dv_in, wide_in.at[3]), (dz_in, wide_in.at[4]), (ao_in, oin.at[0]), (do_in, oin.at[1]),
        (tok_in, tokbuf.at[t, core]), (gain_in, gain), (shift_in, shift), (dlog_in, dlog),
        (sink_src, sink_in), (og_in, og),
    ]
    loads = [pltpu.make_async_copy(a, b, in_sem.at[i]) for i, (a, b) in enumerate(loads)]
    for c in loads:
        c.start()

    ws = Spread(kb, core, z, y, t, wbuf, lambda c: pack.at[c], w_s, w_r)
    os = Spread(kb, core, z, y, t, obuf, lambda c: obuf.at[mine], o_s, o_r)
    bar = pltpu.get_barrier_semaphore()
    pl.semaphore_signal(bar, inc=1, device_id=(partner, t), device_id_type=MESH)
    for d in range(1, nt):
        pl.semaphore_signal(bar, inc=1, device_id=(me, lax.rem(t + d, nt)), device_id_type=MESH)
    for da in (2, 1, -1):
        for axis in (0, 1):
            for c in range(2):
                p = 2 * ws.chip(axis, da, 0) + c
                pl.semaphore_signal(bar, inc=1, device_id=(p, t), device_id_type=MESH)

    for c in loads:
        c.wait()
    gates = [bw[...], gw[...]]
    lines = []
    for c in range(2):
        lines += [g[2 * c : 2 * c + 2].astype(F32) for g in gates]
        lines.append(jnp.zeros((hd - 4, kb), F32))
    gates = jnp.concatenate(lines, axis=0)
    gates = jnp.concatenate([gates, jnp.zeros((2 * hd, 2 * hd - kb), F32)], axis=1)
    gates = gates.T[:kb].astype(BF16)
    packed = []
    for c in range(2):
        half = slice(c * hd, (c + 1) * hd)
        packed.append(jnp.concatenate(
            [wide_in[i][:, half] for i in range(5)] + [slim_in[0], slim_in[1], gates[:, half]], axis=1
        ))
        pack[c] = packed[c]
    wbuf[mine] = jnp.where(core == 0, packed[0], packed[1])
    obuf[mine] = jnp.concatenate(
        [oin[0][:, :hd], oin[1][:, :hd], oin[0][:, hd:], oin[1][:, hd:]], axis=1
    )
    pl.semaphore_wait(bar, 12 + nt)

    ws.begin()

    def tok_copy(k, j, c, device):
        ref = tokbuf.at[j, c]
        return copy_to(ref, ref, tok_s.at[k], tok_r.at[j, c], device)

    tok_copies = [
        tok_copy(d - 1, t, core, (me, lax.rem(t + d, nt))) for d in (1, 3, 2)
    ] + [tok_copy(nt - 1, t, core, (partner, t))]
    for c in tok_copies:
        c.start()
    ws.forward()
    for d in range(1, nt):
        j = lax.rem(t + d, nt)
        tok_copy(0, j, core, (partner, t)).wait_recv()
        c = tok_copy(nt - 1 + d, j, core, (partner, t))
        c.start()
        tok_copies.append(c)

    def norm(c):
        place = pl.ds(pl.multiple_of(c * rows, rows), rows)
        total = jnp.zeros((rows, 1), F32)
        for j in range(nt):
            x = tokbuf[j, c].astype(F32)
            total += jnp.sum(x * x, axis=-1, keepdims=True)
        inverse = lax.rsqrt(total / (nt * width) + norm_eps)
        for j in range(nt):
            cols = slice(j * width, (j + 1) * width)
            normed[place, cols] = (tokbuf[j, c].astype(F32) * inverse * gain[:, cols]).astype(BF16)

    norm(core)
    for j in range(nt):
        tok_copy(0, j, 1 - core, (partner, t)).wait_recv()
    norm(1 - core)
    os.begin()
    ws.finish()

    acc[...] = plain(normed[...], wbuf[...])
    both = 2 * rows
    kvbuf[WINDOW : WINDOW + both] = acc[:, 5 * hd : 7 * hd].astype(BF16)

    @pl.when(chip == 0)
    def _():
        kvbuf[:WINDOW] = jnp.zeros((WINDOW, 2 * hd), BF16)

    @pl.when(chip == chips - 1)
    def _():
        kvbuf[WINDOW + both :] = jnp.zeros((WINDOW, 2 * hd), BF16)

    def halo(p):
        up = copy_to(
            kvbuf.at[pl.ds(both, WINDOW)], kvbuf.at[pl.ds(0, WINDOW)],
            kv_s.at[0], kv_r.at[0], (me + 2, t),
        )
        down = copy_to(
            kvbuf.at[pl.ds(WINDOW, WINDOW)], kvbuf.at[pl.ds(WINDOW + both, WINDOW)],
            kv_s.at[1], kv_r.at[1], (me - 2, t),
        )
        return (up, down)[p]

    pl.when(chip < chips - 1)(lambda: halo(0).start())
    pl.when(chip > 0)(lambda: halo(1).start())
    os.forward()

    lane = lax.broadcasted_iota(jnp.int32, (1, 2 * hd), 1)
    shift_row = jnp.where(lane == hd, shift[0, core], shift[1, core])
    dlog_row = jnp.where(lane == hd + 2, dlog[0, core], dlog[1, core])
    coef = jnp.where((lane == hd + 2) | (lane == hd + 3), -jnp.exp(dlog_row) / (rows * n), 0.0)
    ri = lax.broadcasted_iota(jnp.int32, (rows, rows), 0)
    ci = lax.broadcasted_iota(jnp.int32, (rows, rows), 1)
    incl = (ri >= ci, ri <= ci)
    strict = (ri > ci, ri < ci)
    ones = [jnp.where(m, 1.0, 0.0).astype(F32) for m in incl]
    chains = []
    for j in range(2):
        part_rows = slice(j * rows, (j + 1) * rows)
        tail = acc[part_rows, 6 * hd :]
        soft = jnp.maximum(tail, 0.0) + jnp.log1p(jnp.exp(-jnp.abs(tail)))
        g = coef * soft
        cums = [exact(m, g) for m in ones]
        columns = jnp.where(
            lane == hd + 2, cums[0],
            jnp.where(lane == hd + 3, cums[1], jax.nn.sigmoid(tail + shift_row)),
        )
        lines = columns.T

        def cols(i):
            return acc[part_rows, i * hd : (i + 1) * hd].astype(BF16).astype(F32)

        q = unit_rows(silu(cols(1))) * hd ** (-0.5)
        k = unit_rows(silu(cols(2)))
        v = silu(cols(3))
        kk = near(k, k, ((1,), (1,)))
        qk = near(q, k, ((1,), (1,)))
        for r in range(2):
            at = hd + 2 + r
            gcol = columns[:, at : at + 1]
            grow = lines[at : at + 1, :]
            beta = columns[:, hd + r : hd + r + 1]
            decay = jnp.where(incl[r], jnp.exp(jnp.minimum(gcol - grow, 0.0)), 0.0)
            a = jnp.where(strict[r], beta * kk * decay, 0.0)
            eg = jnp.exp(gcol)
            last = gcol[rows - 1 : rows, :] if r == 0 else gcol[0:1, :]
            chains.append(
                dict(
                    r=r, j=j, a=a, rhs=jnp.concatenate([beta * v, beta * k * eg], axis=1),
                    pm=qk * decay, qe=q * eg, kd=(k * jnp.exp(last - gcol)).T, last=last,
                )
            )
    levels = rows.bit_length() - 1
    eye = jnp.where(ri == ci, 1.0, 0.0).astype(F32)
    xor = ri ^ ci
    inv = [eye - jnp.where(xor == 1, ch["a"], 0.0) for ch in chains]
    pairs = [split(ch["a"]) for ch in chains]
    for lv in range(1, levels):
        m = jnp.where((xor >> lv) == 1, 1.0, 0.0).astype(BF16)
        xs = [split(x) for x in inv]
        left = [close(x, (m * a[0], m * a[1])) for x, a in zip(xs, pairs)]
        inv = [x - close(split(y_), z_) for x, y_, z_ in zip(inv, left, xs)]
    sols = [split(close(split(x), split(ch["rhs"]))) for x, ch in zip(inv, chains)]
    outs = [close(split(ch["kd"]), s) for ch, s in zip(chains, sols)]
    e64 = jnp.where(
        lax.broadcasted_iota(jnp.int32, (hd, hd), 0)
        == lax.broadcasted_iota(jnp.int32, (hd, hd), 1), 1.0, 0.0,
    ).astype(F32)
    moves = [
        jnp.concatenate([s[:, :hd], jnp.exp(ch["last"]) * e64 - s[:, hd:]], axis=1)
        for ch, s in zip(chains, outs)
    ]
    none = jnp.zeros((hd, hd), F32)
    for r in range(2):
        early, late = moves[2 * r + r], moves[2 * (1 - r) + r]
        full = close(split(late[:, hd:]), split(early))
        full += jnp.concatenate([late[:, :hd], none], axis=1)
        st[r] = full.astype(BF16)

    def state_copy(r, p):
        return copy_to(st.at[r], stbuf.at[chip], st_s.at[p], st_r.at[chip], (2 * p + core, t))

    def state_all(act):
        for d in range(1, chips):
            pl.when(chip + d < chips)(lambda d=d: act(state_copy(0, chip + d)))
            pl.when(chip - d >= 0)(lambda d=d: act(state_copy(1, chip - d)))

    state_all(lambda c: c.start())
    inner = [close(split(ch["pm"]), s) for ch, s in zip(chains, sols)]
    for ch, s in zip(chains, inner):
        o_loc[ch["j"], ch["r"]] = s[:, :hd]
        r_mat[ch["j"], ch["r"]] = ch["qe"] - s[:, hd:]

    pl.when(chip > 0)(lambda: halo(0).wait_recv())
    pl.when(chip < chips - 1)(lambda: halo(1).wait_recv())
    span = rows + 2 * WINDOW
    qi = lax.broadcasted_iota(jnp.int32, (rows, span), 0)
    kj = lax.broadcasted_iota(jnp.int32, (rows, span), 1) - WINDOW
    sink = sink_in[core]
    for j in range(2):
        pos = kj + (2 * chip + j) * rows
        allowed = (jnp.abs(qi - kj) <= WINDOW) & (pos >= 0) & (pos < n * rows)
        q = acc[j * rows : (j + 1) * rows, :hd].astype(BF16)
        keys = slice(j * rows, j * rows + span)
        s = plain(q, kvbuf[keys, :hd], ((1,), (1,))) * hd ** (-0.5)
        s = jnp.where(allowed, s, -jnp.inf)
        m = jnp.maximum(jnp.max(s, axis=-1, keepdims=True), sink)
        e = jnp.exp(s - m)
        p = e / (jnp.sum(e, axis=-1, keepdims=True) + jnp.exp(sink - m))
        heads[j, :, :hd] = plain(p.astype(BF16), kvbuf[keys, hd:]).astype(BF16)

    ident = jnp.concatenate([none, e64], axis=1).astype(BF16)
    sums, prods = [none, none], [e64, e64]
    for d in range(1, chips):
        for r in range(2):
            there = chip - d if r == 0 else chip + d
            ok = there >= 0 if r == 0 else there < chips

            @pl.when(ok)
            def _(there=there):
                copy_to(st.at[0], stbuf.at[there], st_s.at[0], st_r.at[there], (me, t)).wait_recv()

            move = jnp.where(ok, stbuf[jnp.where(ok, there, chip)], ident)
            high, low = split(prods[r])
            step = plain(jnp.concatenate([high, low], axis=1), jnp.concatenate([move, move], axis=0))
            sums[r] = sums[r] + step[:, :hd]
            prods[r] = step[:, hd:]
    for j in range(2):
        o = o_loc[j, 0] + o_loc[j, 1]
        for r in range(2):
            state = sums[r]
            if j != r:
                prev = moves[2 * (1 - j) + r]
                state = near(prev[:, hd:], state) + prev[:, :hd]
            o += near(r_mat[j, r], state)
        o = o * lax.rsqrt(jnp.mean(o * o, axis=-1, keepdims=True) + norm_eps) * og[...]
        gate = acc[j * rows : (j + 1) * rows, 4 * hd : 5 * hd].astype(BF16).astype(F32)
        heads[j, :, hd:] = (o * silu(gate)).astype(BF16)

    hand = copy_to(heads.at[1 - core], other, h_s, h_r, (partner, t))
    hand.start()
    os.finish()
    tr = rows // nt
    side = lambda c: obuf[:, pl.ds(pl.multiple_of(c * 2 * hd, 2 * hd), 2 * hd)]
    result = plain(heads[core], side(core), ((1,), (1,)))
    hand.wait_recv()
    result += plain(other[...], side(1 - core), ((1,), (1,)))
    for j in range(nt):
        part[j] = result[j * tr : (j + 1) * tr].astype(SUM_DTYPE)
    rs_copies = [
        copy_to(
            part.at[lax.rem(t + d, nt)], rsbuf.at[d - 1], rs_s.at[d - 1], rs_r.at[d - 1],
            (me, lax.rem(t + d, nt)),
        )
        for d in range(1, nt)
    ]
    for c in rs_copies:
        c.start()
    for c in tok_copies:
        c.wait_send()
    ws.drain()
    os.drain()
    pl.when(chip < chips - 1)(lambda: halo(0).wait_send())
    pl.when(chip > 0)(lambda: halo(1).wait_send())
    state_all(lambda c: c.wait_send())
    hand.wait_send()
    total = part[t].astype(F32)
    for d in range(1, nt):
        rs_copies[d - 1].wait_recv()
        total += rsbuf[d - 1].astype(F32)
    out[...] = total.astype(BF16)
    for c in rs_copies:
        c.wait_send()


def per_device(
    tokens, norm_gain, attn_query, attn_key, attn_value, sink_logit, delta_query, delta_key,
    delta_value, delta_gate, beta_weight, decay_weight, beta_shift, decay_log, out_gain,
    attn_out, delta_out,
):
    n, nt = lax.axis_size("sp"), lax.axis_size("tp")
    rows, width = tokens.shape
    kb = attn_query.shape[0]
    hd = HEAD_DIM
    cw = attn_out.shape[1]
    tr = rows // nt
    chips = n // 2
    assert n == 2 * RING * RING and cw == kb and rows == 2 * hd
    assert attn_query.shape[1] == delta_query.shape[1] == 2 * attn_key.shape[1] == 2 * hd
    gates = lambda w: jnp.transpose(w, (1, 2, 0)).reshape(4, kb)
    dma = pltpu.SemaphoreType.DMA
    vm, sm = pltpu.VMEM, pltpu.SMEM
    hbm = pl.BlockSpec(memory_space=pltpu.HBM)
    return pl.pallas_call(
        functools.partial(layer_kernel, n, nt),
        out_shape=jax.ShapeDtypeStruct((tr, n * cw), BF16),
        in_specs=[hbm] * 17,
        out_specs=pl.BlockSpec(memory_space=pltpu.VMEM),
        scratch_shapes=[
            vm((1, nt * width), F32),
            vm((5, kb, 2 * hd), BF16),
            vm((2, kb, hd), BF16),
            vm((2, cw, 2 * hd), BF16),
            vm((4, kb), BF16),
            vm((4, kb), BF16),
            sm((2, 2), F32),
            sm((2, 2), F32),
            sm((2,), F32),
            vm((1, hd), F32),
            dma((17,)),
            vm((nt, 2, rows, width), BF16),
            vm((2 * rows, nt * width), BF16),
            vm((2, kb, 8 * hd), BF16),
            vm((n * kb, 8 * hd), BF16),
            vm((n * cw, 4 * hd), BF16),
            vm((2 * rows, 8 * hd), F32),
            vm((2 * rows + 2 * WINDOW, 2 * hd), BF16),
            vm((2, hd, 2 * hd), BF16),
            vm((chips, hd, 2 * hd), BF16),
            vm((2, 2, rows, hd), F32),
            vm((2, 2, rows, hd), F32),
            vm((2, rows, 2 * hd), BF16),
            vm((rows, 2 * hd), BF16),
            vm((nt, tr, n * cw), SUM_DTYPE),
            vm((nt - 1, tr, n * cw), SUM_DTYPE),
            dma((2 * nt - 1,)), dma((nt, 2)),
            dma((n - 1,)), dma((n,)),
            dma((n - 1,)), dma((n,)),
            dma((2,)), dma((2,)),
            dma((chips,)), dma((chips,)),
            dma, dma,
            dma((nt - 1,)), dma((nt - 1,)),
        ],
        compiler_params=pltpu.CompilerParams(
            collective_id=0, has_side_effects=True, vmem_limit_bytes=67043328
        ),
    )(
        tokens, norm_gain.reshape(1, nt * width), attn_query, attn_key, attn_value, delta_query,
        delta_key, delta_value, delta_gate, attn_out.T, delta_out.T, gates(beta_weight),
        gates(decay_weight), beta_shift, decay_log, sink_logit, out_gain.reshape(1, hd),
    )


def solution(mesh):
    return jax.shard_map(
        per_device,
        mesh=mesh,
        in_specs=(
            P("sp", "tp"), P(), P("sp", "tp"), P("sp", "tp"), P("sp", "tp"), P("tp"),
            P("sp", "tp"), P("sp", "tp"), P("sp", "tp"), P("sp", "tp"),
            P("sp", "tp", None), P("sp", "tp", None), P(None, "tp"), P(None, "tp"), P(),
            P("tp", "sp"), P("tp", "sp"),
        ),
        out_specs=P(("sp", "tp"), None),
        check_vma=False,
    )
```

time: 69.5 us -> 45 us (0.65)
  Pallas kernels: 58.3 us -> 43.3 us
  local copies, waits for them, and re-layouts: 10.4 us -> 1.47 us
    pallas_call x1, Pallas kernels: 58.3 us -> 43.3 us  [per_device(): pl.pallas_call(functools.partial(layer_kernel, n, nt), out_shape=jax.Shap...]
    unnamed x35 -> x1, local copies, waits for them, and re-layouts: 10.4 us -> 1.47 us
where the time goes in v2:
time: 45 us; the launch traced here: 44.8 us
  Pallas kernels  43.3 us (96%)
  local copies, waits for them, and re-layouts  1.47 us (3%)
    pallas_call x1, Pallas kernels, per_device(): pl.pallas_call(functools.partial(layer_kernel, n, nt), out_shape=jax.Shap...  43.3 us
    unnamed x1, local copies, waits for them, and re-layouts  1.47 us

profile of v2, /device:TPU:1, one launch (start us, length us, event | category | flops | bytes accessed | tf_op | source)
XLA Modules:
  0.0 44.8 jit_solution(3739967602367251994)
XLA Ops:
  0.0 43.3 %shard_map.163 = bf16[32,1024]{1,0:T(8,128)(2,1)} custom-call(bf16[128,256]{1,0:T(8,128)(2,1)} %tok_in.1, f32[1,1024]{1,0:T(1,128)} %bitcast.12, bf16[32,128]{1,0:T(8,128)(2,1)} %aq_in.1, bf16[32,64]{1,0:T(8,128)(2,1)} %ak_in.1, bf16[32,64]{1,0:T(8,128)(2,1)} %av_in.1, bf16[32,128]{1,0:T(8,128)(2,1)} %dq_in.1, bf16[32,128]{1,0:T(8,128)(2,1)} %dk_in.1, ...), custom_call_target="tpu_custom_call" | custom-call | tf_op jit(solution)/shard_map/pallas_call | solution.py:432
  43.3 1.5 %copy.19 = bf16[32,1024]{1,0:T(8,128)(2,1)} copy(bf16[32,1024]{1,0:T(8,128)(2,1)} %shard_map.163) | data formatting | bytes 131072

commit v3 on v2

--- a/solution.py
+++ b/solution.py
@@ -13,7 +13,6 @@
 MESH = pl.DeviceIdType.MESH
 F32 = jnp.float32
 BF16 = jnp.bfloat16
-SUM_DTYPE = jnp.bfloat16
 RING = 4
 
 
@@ -64,51 +63,55 @@
 
 
 class Spread:
-    def __init__(self, kb, core, z, y, t, buf, own, send_sem, recv_sem):
-        self.kb, self.core, self.z, self.y, self.t = kb, core, z, y, t
-        self.buf, self.own, self.send_sem, self.recv_sem = buf, own, send_sem, recv_sem
+    def __init__(self, core, z, y, t, rows, own, send_sem, recv_sem, single=False):
+        self.core, self.z, self.y, self.t = core, z, y, t
+        self.rows, self.own, self.send_sem, self.recv_sem = rows, own, send_sem, recv_sem
+        self.single, self.axes = single, (core,) if single else (0, 1)
+        self.partner = 2 * (z * RING + y) + 1 - core
         self.started = []
 
     def chip(self, axis, da, db):
-        dz, dy = (db, da) if axis == 0 else (da, db)
+        dz, dy = db + axis * (da - db), da + axis * (db - da)
         return lax.rem(self.z + dz + RING, RING) * RING + lax.rem(self.y + dy + RING, RING)
 
     def send(self, src, blk, device):
         k = len(self.started)
-        dst = self.buf.at[pl.ds(blk * self.kb, self.kb)]
-        c = copy_to(src, dst, self.send_sem.at[k], self.recv_sem.at[blk], (device, self.t))
+        c = copy_to(src, self.rows(blk), self.send_sem.at[k], self.recv_sem.at[blk], (device, self.t))
         c.start()
         self.started.append(c)
 
     def landed(self, blk):
-        ref = self.buf.at[pl.ds(blk * self.kb, self.kb)]
-        partner = 2 * (self.z * RING + self.y) + 1 - self.core
-        copy_to(ref, ref, self.send_sem.at[0], self.recv_sem.at[blk], (partner, self.t)).wait_recv()
+        ref = self.rows(blk)
+        copy_to(ref, ref, self.send_sem.at[0], self.recv_sem.at[blk], (self.partner, self.t)).wait_recv()
 
     def begin(self):
         me = 2 * self.chip(0, 0, 0) + self.core
         for da in (2, 1, -1):
             for axis in (0, 1):
-                to = self.chip(axis, da, 0)
-                for c in range(2):
-                    self.send(self.own(c), me, 2 * to + c)
-        self.send(self.own(1 - self.core), me, me + 1 - 2 * self.core)
+                to = 2 * self.chip(axis, da, 0)
+                if self.single:
+                    self.send(self.own(self.core), me, to + self.core)
+                else:
+                    for c in range(2):
+                        self.send(self.own(c), me, to + c)
+        if not self.single:
+            self.send(self.own(1 - self.core), me, self.partner)
 
     def forward(self):
         for r in (1, -1, 2):
-            for axis in (0, 1):
+            for axis in self.axes:
                 blk = 2 * self.chip(axis, r, 0) + axis
                 self.landed(blk)
                 for db in (2, 1, -1):
-                    src = self.buf.at[pl.ds(blk * self.kb, self.kb)]
-                    self.send(src, blk, 2 * self.chip(axis, 0, db) + self.core)
+                    self.send(self.rows(blk), blk, 2 * self.chip(axis, 0, db) + self.core)
 
     def finish(self):
-        self.landed(2 * self.chip(0, 0, 0) + 1 - self.core)
-        for axis in (0, 1):
-            for r in (0, 1, -1, 2):
+        for r in (0, 1, -1, 2):
+            for axis in self.axes:
                 for db in (1, -1, 2):
                     self.landed(2 * self.chip(axis, r, db) + axis)
+        if not self.single:
+            self.landed(self.partner)
 
     def drain(self):
         for c in self.started:
@@ -120,8 +123,8 @@
     tok_in, gain_in, aq_in, ak_in, av_in, dq_in, dk_in, dv_in, dz_in, ao_in, do_in, bw_in, gw_in,
     shift_in, dlog_in, sink_src, og_in, out,
     gain, wide_in, slim_in, oin, bw, gw, shift, dlog, sink_in, og, in_sem,
-    tokbuf, normed, pack, wbuf, obuf, acc, kvbuf, st, stbuf, o_loc, r_mat, heads, other, part, rsbuf,
-    tok_s, tok_r, w_s, w_r, o_s, o_r, kv_s, kv_r, st_s, st_r, h_s, h_r, rs_s, rs_r,
+    tokbuf, normed, pack1, pack2, wbuf1, wbuf2, obuf, acc1, acc2, kvbuf, st, stbuf, o_loc, r_mat, heads, gath,
+    tok_s, tok_r, w1_s, w1_r, w2_s, w2_r, x_s, x_r, g_s, g_r, o_s, o_r, kv_s, kv_r, st_s, st_r, h_s, h_r,
 ):
     me, t = lax.axis_index("sp"), lax.axis_index("tp")
     rows, width = tok_in.shape
@@ -144,8 +147,12 @@
     for c in loads:
         c.start()
 
-    ws = Spread(kb, core, z, y, t, wbuf, lambda c: pack.at[c], w_s, w_r)
-    os = Spread(kb, core, z, y, t, obuf, lambda c: obuf.at[mine], o_s, o_r)
+    feats = lambda i: pl.ds(pl.multiple_of(i * 4 * hd, 4 * hd), 4 * hd)
+    rows_of = lambda buf: lambda blk: buf.at[pl.ds(blk * kb, kb)]
+    o_rows = lambda blk: obuf.at[lax.div(blk, 2), lax.rem(blk, 2), :, feats(t)]
+    w1 = Spread(core, z, y, t, rows_of(wbuf1), lambda c: pack1.at[c], w1_s, w1_r)
+    w2 = Spread(core, z, y, t, rows_of(wbuf2), lambda c: pack2.at[c], w2_s, w2_r)
+    os = Spread(core, z, y, t, o_rows, lambda c: o_rows(me), o_s, o_r, single=True)
     bar = pltpu.get_barrier_semaphore()
     pl.semaphore_signal(bar, inc=1, device_id=(partner, t), device_id_type=MESH)
     for d in range(1, nt):
@@ -153,7 +160,7 @@
     for da in (2, 1, -1):
         for axis in (0, 1):
             for c in range(2):
-                p = 2 * ws.chip(axis, da, 0) + c
+                p = 2 * w1.chip(axis, da, 0) + c
                 pl.semaphore_signal(bar, inc=1, device_id=(p, t), device_id_type=MESH)
 
     for c in loads:
@@ -166,20 +173,22 @@
     gates = jnp.concatenate(lines, axis=0)
     gates = jnp.concatenate([gates, jnp.zeros((2 * hd, 2 * hd - kb), F32)], axis=1)
     gates = gates.T[:kb].astype(BF16)
-    packed = []
+    packs = ([], [])
     for c in range(2):
         half = slice(c * hd, (c + 1) * hd)
-        packed.append(jnp.concatenate(
-            [wide_in[i][:, half] for i in range(5)] + [slim_in[0], slim_in[1], gates[:, half]], axis=1
-        ))
-        pack[c] = packed[c]
-    wbuf[mine] = jnp.where(core == 0, packed[0], packed[1])
-    obuf[mine] = jnp.concatenate(
+        aq, dq, dk, dv, dz = [wide_in[i][:, half] for i in range(5)]
+        packs[0].append(jnp.concatenate([dk, dv, dq, gates[:, half]], axis=1))
+        packs[1].append(jnp.concatenate([aq, dz, slim_in[0], slim_in[1]], axis=1))
+        pack1[c], pack2[c] = packs[0][c], packs[1][c]
+    wbuf1[mine] = jnp.where(core == 0, packs[0][0], packs[0][1])
+    wbuf2[mine] = jnp.where(core == 0, packs[1][0], packs[1][1])
+    obuf[chip, core, :, feats(t)] = jnp.concatenate(
         [oin[0][:, :hd], oin[1][:, :hd], oin[0][:, hd:], oin[1][:, hd:]], axis=1
     )
     pl.semaphore_wait(bar, 12 + nt)
 
-    ws.begin()
+    w1.begin()
+    w2.begin()
 
     def tok_copy(k, j, c, device):
         ref = tokbuf.at[j, c]
@@ -190,7 +199,11 @@
     ] + [tok_copy(nt - 1, t, core, (partner, t))]
     for c in tok_copies:
         c.start()
-    ws.forward()
+
+    os.begin()
+    w1.forward()
+    w2.forward()
+    os.forward()
     for d in range(1, nt):
         j = lax.rem(t + d, nt)
         tok_copy(0, j, core, (partner, t)).wait_recv()
@@ -213,35 +226,24 @@
     for j in range(nt):
         tok_copy(0, j, 1 - core, (partner, t)).wait_recv()
     norm(1 - core)
-    os.begin()
-    ws.finish()
-
-    acc[...] = plain(normed[...], wbuf[...])
-    both = 2 * rows
-    kvbuf[WINDOW : WINDOW + both] = acc[:, 5 * hd : 7 * hd].astype(BF16)
-
-    @pl.when(chip == 0)
-    def _():
-        kvbuf[:WINDOW] = jnp.zeros((WINDOW, 2 * hd), BF16)
-
-    @pl.when(chip == chips - 1)
-    def _():
-        kvbuf[WINDOW + both :] = jnp.zeros((WINDOW, 2 * hd), BF16)
-
-    def halo(p):
-        up = copy_to(
-            kvbuf.at[pl.ds(both, WINDOW)], kvbuf.at[pl.ds(0, WINDOW)],
-            kv_s.at[0], kv_r.at[0], (me + 2, t),
-        )
-        down = copy_to(
-            kvbuf.at[pl.ds(WINDOW, WINDOW)], kvbuf.at[pl.ds(WINDOW + both, WINDOW)],
-            kv_s.at[1], kv_r.at[1], (me - 2, t),
-        )
-        return (up, down)[p]
-
-    pl.when(chip < chips - 1)(lambda: halo(0).start())
-    pl.when(chip > 0)(lambda: halo(1).start())
-    os.forward()
+    w1.finish()
+
+    acc1[...] = plain(normed[...], wbuf1[...])
+    os.finish()
+
+    def x_copy(k, j, device):
+        ref = obuf.at[:, core, :, feats(j)]
+        return copy_to(ref, ref, x_s.at[k], x_r.at[j], (me, device))
+
+    x_copies = [x_copy(d - 1, t, lax.rem(t + d, nt)) for d in range(1, nt)]
+    for c in x_copies:
+        c.start()
+
+    def share(j, c):
+        ref = obuf.at[:, c, :, feats(j)]
+        return copy_to(ref, ref, g_s.at[j], g_r.at[j], (partner, t))
+
+    share(t, core).start()
 
     lane = lax.broadcasted_iota(jnp.int32, (1, 2 * hd), 1)
     shift_row = jnp.where(lane == hd, shift[0, core], shift[1, core])
@@ -255,7 +257,7 @@
     chains = []
     for j in range(2):
         part_rows = slice(j * rows, (j + 1) * rows)
-        tail = acc[part_rows, 6 * hd :]
+        tail = acc1[part_rows, 2 * hd :]
         soft = jnp.maximum(tail, 0.0) + jnp.log1p(jnp.exp(-jnp.abs(tail)))
         g = coef * soft
         cums = [exact(m, g) for m in ones]
@@ -266,11 +268,11 @@
         lines = columns.T
 
         def cols(i):
-            return acc[part_rows, i * hd : (i + 1) * hd].astype(BF16).astype(F32)
-
-        q = unit_rows(silu(cols(1))) * hd ** (-0.5)
-        k = unit_rows(silu(cols(2)))
-        v = silu(cols(3))
+            return acc1[part_rows, i * hd : (i + 1) * hd].astype(BF16).astype(F32)
+
+        q = unit_rows(silu(cols(2))) * hd ** (-0.5)
+        k = unit_rows(silu(cols(0)))
+        v = silu(cols(1))
         kk = near(k, k, ((1,), (1,)))
         qk = near(q, k, ((1,), (1,)))
         for r in range(2):
@@ -324,6 +326,32 @@
             pl.when(chip - d >= 0)(lambda d=d: act(state_copy(1, chip - d)))
 
     state_all(lambda c: c.start())
+    w2.finish()
+    acc2[...] = plain(normed[...], wbuf2[...])
+    both = 2 * rows
+    kvbuf[WINDOW : WINDOW + both] = acc2[:, 2 * hd :].astype(BF16)
+
+    @pl.when(chip == 0)
+    def _():
+        kvbuf[:WINDOW] = jnp.zeros((WINDOW, 2 * hd), BF16)
+
+    @pl.when(chip == chips - 1)
+    def _():
+        kvbuf[WINDOW + both :] = jnp.zeros((WINDOW, 2 * hd), BF16)
+
+    def halo(p):
+        up = copy_to(
+            kvbuf.at[pl.ds(both, WINDOW)], kvbuf.at[pl.ds(0, WINDOW)],
+            kv_s.at[0], kv_r.at[0], (me + 2, t),
+        )
+        down = copy_to(
+            kvbuf.at[pl.ds(WINDOW, WINDOW)], kvbuf.at[pl.ds(WINDOW + both, WINDOW)],
+            kv_s.at[1], kv_r.at[1], (me - 2, t),
+        )
+        return (up, down)[p]
+
+    pl.when(chip < chips - 1)(lambda: halo(0).start())
+    pl.when(chip > 0)(lambda: halo(1).start())
     inner = [close(split(ch["pm"]), s) for ch, s in zip(chains, sols)]
     for ch, s in zip(chains, inner):
         o_loc[ch["j"], ch["r"]] = s[:, :hd]
@@ -338,7 +366,7 @@
     for j in range(2):
         pos = kj + (2 * chip + j) * rows
         allowed = (jnp.abs(qi - kj) <= WINDOW) & (pos >= 0) & (pos < n * rows)
-        q = acc[j * rows : (j + 1) * rows, :hd].astype(BF16)
+        q = acc2[j * rows : (j + 1) * rows, :hd].astype(BF16)
         keys = slice(j * rows, j * rows + span)
         s = plain(q, kvbuf[keys, :hd], ((1,), (1,))) * hd ** (-0.5)
         s = jnp.where(allowed, s, -jnp.inf)
@@ -372,42 +400,44 @@
                 state = near(prev[:, hd:], state) + prev[:, :hd]
             o += near(r_mat[j, r], state)
         o = o * lax.rsqrt(jnp.mean(o * o, axis=-1, keepdims=True) + norm_eps) * og[...]
-        gate = acc[j * rows : (j + 1) * rows, 4 * hd : 5 * hd].astype(BF16).astype(F32)
+        gate = acc2[j * rows : (j + 1) * rows, hd : 2 * hd].astype(BF16).astype(F32)
         heads[j, :, hd:] = (o * silu(gate)).astype(BF16)
 
-    hand = copy_to(heads.at[1 - core], other, h_s, h_r, (partner, t))
-    hand.start()
-    os.finish()
     tr = rows // nt
-    side = lambda c: obuf[:, pl.ds(pl.multiple_of(c * 2 * hd, 2 * hd), 2 * hd)]
-    result = plain(heads[core], side(core), ((1,), (1,)))
-    hand.wait_recv()
-    result += plain(other[...], side(1 - core), ((1,), (1,)))
+    spot = lambda x: pl.ds(pl.multiple_of(x * tr, tr), tr)
+    peers = [(lax.rem(t + d, nt), c) for d in range(1, nt) for c in (core, 1 - core)]
+    peers.append((t, 1 - core))
+
+    def hand(k, x, c):
+        return copy_to(
+            heads.at[c, spot(x)], gath.at[2 * t + core], h_s.at[k], h_r.at[2 * t + core], (2 * chip + c, x)
+        )
+
+    hands = [hand(k, x, c) for k, (x, c) in enumerate(peers)]
+    for c in hands:
+        c.start()
+    gath[2 * t + core] = heads[core, spot(t)]
+    for c in tok_copies + x_copies:
+        c.wait_send()
+    w1.drain()
+    w2.drain()
+    os.drain()
+    for d in range(1, nt):
+        j = lax.rem(t + d, nt)
+        x_copy(0, j, j).wait_recv()
+        share(j, core).start()
     for j in range(nt):
-        part[j] = result[j * tr : (j + 1) * tr].astype(SUM_DTYPE)
-    rs_copies = [
-        copy_to(
-            part.at[lax.rem(t + d, nt)], rsbuf.at[d - 1], rs_s.at[d - 1], rs_r.at[d - 1],
-            (me, lax.rem(t + d, nt)),
-        )
-        for d in range(1, nt)
-    ]
-    for c in rs_copies:
-        c.start()
-    for c in tok_copies:
-        c.wait_send()
-    ws.drain()
-    os.drain()
+        share(j, core).wait_send()
+        share(j, 1 - core).wait_recv()
     pl.when(chip < chips - 1)(lambda: halo(0).wait_send())
     pl.when(chip > 0)(lambda: halo(1).wait_send())
     state_all(lambda c: c.wait_send())
-    hand.wait_send()
-    total = part[t].astype(F32)
-    for d in range(1, nt):
-        rs_copies[d - 1].wait_recv()
-        total += rsbuf[d - 1].astype(F32)
-    out[...] = total.astype(BF16)
-    for c in rs_copies:
+    for x, c in peers:
+        ref = gath.at[2 * x + c]
+        copy_to(ref, ref, h_s.at[0], h_r.at[2 * x + c], (2 * chip + c, x)).wait_recv()
+    lhs = jnp.concatenate([gath[i] for i in range(2 * nt)], axis=1)
+    out[...] = plain(lhs, obuf[...].reshape(n * kb, -1), ((1,), (1,))).astype(BF16)
+    for c in hands:
         c.wait_send()
 
 
@@ -448,35 +478,38 @@
             dma((17,)),
             vm((nt, 2, rows, width), BF16),
             vm((2 * rows, nt * width), BF16),
-            vm((2, kb, 8 * hd), BF16),
-            vm((n * kb, 8 * hd), BF16),
-            vm((n * cw, 4 * hd), BF16),
-            vm((2 * rows, 8 * hd), F32),
+            vm((2, kb, 4 * hd), BF16),
+            vm((2, kb, 4 * hd), BF16),
+            vm((n * kb, 4 * hd), BF16),
+            vm((n * kb, 4 * hd), BF16),
+            vm((chips, 2, cw, nt * 4 * hd), BF16),
+            vm((2 * rows, 4 * hd), F32),
+            vm((2 * rows, 4 * hd), F32),
             vm((2 * rows + 2 * WINDOW, 2 * hd), BF16),
             vm((2, hd, 2 * hd), BF16),
             vm((chips, hd, 2 * hd), BF16),
             vm((2, 2, rows, hd), F32),
             vm((2, 2, rows, hd), F32),
             vm((2, rows, 2 * hd), BF16),
-            vm((rows, 2 * hd), BF16),
-            vm((nt, tr, n * cw), SUM_DTYPE),
-            vm((nt - 1, tr, n * cw), SUM_DTYPE),
+            vm((2 * nt, tr, 2 * hd), BF16),
             dma((2 * nt - 1,)), dma((nt, 2)),
             dma((n - 1,)), dma((n,)),
             dma((n - 1,)), dma((n,)),
+            dma((nt - 1,)), dma((nt,)),
+            dma((nt,)), dma((nt,)),
+            dma((n - 1,)), dma((n,)),
             dma((2,)), dma((2,)),
             dma((chips,)), dma((chips,)),
-            dma, dma,
-            dma((nt - 1,)), dma((nt - 1,)),
+            dma((2 * nt - 1,)), dma((2 * nt,)),
         ],
         compiler_params=pltpu.CompilerParams(
-            collective_id=0, has_side_effects=True, vmem_limit_bytes=67043328
+            collective_id=0, has_side_effects=True, vmem_limit_bytes=48*1024*1024
         ),
-    )(
+    )(*[pltpu.with_memory_space_constraint(x, pltpu.HBM) for x in (
         tokens, norm_gain.reshape(1, nt * width), attn_query, attn_key, attn_value, delta_query,
         delta_key, delta_value, delta_gate, attn_out.T, delta_out.T, gates(beta_weight),
         gates(decay_weight), beta_shift, decay_log, sink_logit, out_gain.reshape(1, hd),
-    )
+    )])
 
 
 def solution(mesh):

time: 45 us -> 41.8 us (0.929)
  Pallas kernels: 43.3 us -> 41 us
  local copies, waits for them, and re-layouts: 1.47 us -> 0.63 us
    pallas_call x1, Pallas kernels: 43.3 us -> 41 us  [per_device(): pl.pallas_call(functools.partial(layer_kernel, n, nt), out_shape=jax.Shap...]
    unnamed x1, local copies, waits for them, and re-layouts: 1.47 us -> 0.63 us
where the time goes in v3:
time: 41.8 us; the launch traced here: 41.6 us
  Pallas kernels  41 us (98%)
  local copies, waits for them, and re-layouts  0.63 us (2%)
    pallas_call x1, Pallas kernels, per_device(): pl.pallas_call(functools.partial(layer_kernel, n, nt), out_shape=jax.Shap...  41 us

profile of v3, /device:TPU:1, one launch (start us, length us, event | category | flops | bytes accessed | tf_op | source)
XLA Modules:
  0.0 41.6 jit_solution(2216731573792158369)
XLA Ops:
  0.0 41.0 %shard_map.163 = bf16[32,1024]{1,0:T(8,128)(2,1)S(1)} custom-call(bf16[128,256]{1,0:T(8,128)(2,1)} %tok_in.1, f32[1,1024]{1,0:T(1,128)} %bitcast.12, bf16[32,128]{1,0:T(8,128)(2,1)} %aq_in.1, bf16[32,64]{1,0:T(8,128)(2,1)} %ak_in.1, bf16[32,64]{1,0:T(8,128)(2,1)} %av_in.1, bf16[32,128]{1,0:T(8,128)(2,1)} %dq_in.1, bf16[32,128]{1,0:T(8,128)(2,1)} %dk_in.1, ...), custom_call_target="tpu_custom_call" | custom-call | tf_op jit(solution)/shard_map/pallas_call | solution.py:462
  41.0 0.6 %copy.19 = bf16[32,1024]{1,0:T(8,128)(2,1)} copy(bf16[32,1024]{1,0:T(8,128)(2,1)S(1)} %shard_map.163) | data formatting | bytes 131072

commit v4 on v3

--- a/solution.py
+++ b/solution.py
@@ -105,10 +105,10 @@
                 for db in (2, 1, -1):
                     self.send(self.rows(blk), blk, 2 * self.chip(axis, 0, db) + self.core)
 
-    def finish(self):
+    def finish(self, dbs=(1, -1, 2)):
         for r in (0, 1, -1, 2):
             for axis in self.axes:
-                for db in (1, -1, 2):
+                for db in dbs:
                     self.landed(2 * self.chip(axis, r, db) + axis)
         if not self.single:
             self.landed(self.partner)
@@ -149,7 +149,7 @@
 
     feats = lambda i: pl.ds(pl.multiple_of(i * 4 * hd, 4 * hd), 4 * hd)
     rows_of = lambda buf: lambda blk: buf.at[pl.ds(blk * kb, kb)]
-    o_rows = lambda blk: obuf.at[lax.div(blk, 2), lax.rem(blk, 2), :, feats(t)]
+    o_rows = lambda blk: obuf.at[lax.div(blk, 2 * RING), lax.rem(lax.div(blk, 2), RING), lax.rem(blk, 2), :, feats(t)]
     w1 = Spread(core, z, y, t, rows_of(wbuf1), lambda c: pack1.at[c], w1_s, w1_r)
     w2 = Spread(core, z, y, t, rows_of(wbuf2), lambda c: pack2.at[c], w2_s, w2_r)
     os = Spread(core, z, y, t, o_rows, lambda c: o_rows(me), o_s, o_r, single=True)
@@ -182,13 +182,12 @@
         pack1[c], pack2[c] = packs[0][c], packs[1][c]
     wbuf1[mine] = jnp.where(core == 0, packs[0][0], packs[0][1])
     wbuf2[mine] = jnp.where(core == 0, packs[1][0], packs[1][1])
-    obuf[chip, core, :, feats(t)] = jnp.concatenate(
+    obuf[z, y, core, :, feats(t)] = jnp.concatenate(
         [oin[0][:, :hd], oin[1][:, :hd], oin[0][:, hd:], oin[1][:, hd:]], axis=1
     )
     pl.semaphore_wait(bar, 12 + nt)
 
     w1.begin()
-    w2.begin()
 
     def tok_copy(k, j, c, device):
         ref = tokbuf.at[j, c]
@@ -201,9 +200,8 @@
         c.start()
 
     os.begin()
+    w2.begin()
     w1.forward()
-    w2.forward()
-    os.forward()
     for d in range(1, nt):
         j = lax.rem(t + d, nt)
         tok_copy(0, j, core, (partner, t)).wait_recv()
@@ -226,25 +224,39 @@
     for j in range(nt):
         tok_copy(0, j, 1 - core, (partner, t)).wait_recv()
     norm(1 - core)
+    w2.forward()
+    os.forward()
+
+    def own_class(act):
+        for c in range(2):
+            pl.when(core == c)(lambda c=c: act(c))
+
+    def band(db, c, cols):
+        if c == 0:
+            return obuf.at[lax.rem(z + db, RING), :, 0, :, cols]
+        return obuf.at[:, lax.rem(y + db, RING), 1, :, cols]
+
+    def x_copy(db, d, c, j):
+        ref = band(db, c, feats(j))
+        return copy_to(ref, ref, x_s.at[db, d - 1], x_r.at[db, j], (me, lax.rem(t + d, nt)))
+
+    def x_all(db, act):
+        for d in range(1, nt):
+            own_class(lambda c, d=d: act(x_copy(db, d, c, t)))
+
+    def share(db, c):
+        ref = band(db, c, pl.ds(0, nt * 4 * hd))
+        return copy_to(ref, ref, g_s.at[db], g_r.at[db], (partner, t))
+
+    def pass_on(db):
+        for d in range(1, nt):
+            own_class(lambda c, d=d: x_copy(db, d, c, lax.rem(t + d, nt)).wait_recv())
+        own_class(lambda c: share(db, c).start())
+
+    x_all(0, lambda c: c.start())
     w1.finish()
 
     acc1[...] = plain(normed[...], wbuf1[...])
-    os.finish()
-
-    def x_copy(k, j, device):
-        ref = obuf.at[:, core, :, feats(j)]
-        return copy_to(ref, ref, x_s.at[k], x_r.at[j], (me, device))
-
-    x_copies = [x_copy(d - 1, t, lax.rem(t + d, nt)) for d in range(1, nt)]
-    for c in x_copies:
-        c.start()
-
-    def share(j, c):
-        ref = obuf.at[:, c, :, feats(j)]
-        return copy_to(ref, ref, g_s.at[j], g_r.at[j], (partner, t))
-
-    share(t, core).start()
-
     lane = lax.broadcasted_iota(jnp.int32, (1, 2 * hd), 1)
     shift_row = jnp.where(lane == hd, shift[0, core], shift[1, core])
     dlog_row = jnp.where(lane == hd + 2, dlog[0, core], dlog[1, core])
@@ -317,6 +329,9 @@
         full += jnp.concatenate([late[:, :hd], none], axis=1)
         st[r] = full.astype(BF16)
 
+    for db in (1, 3, 2):
+        os.finish((db if db < 3 else -1,))
+        x_all(db, lambda c: c.start())
     def state_copy(r, p):
         return copy_to(st.at[r], stbuf.at[chip], st_s.at[p], st_r.at[chip], (2 * p + core, t))
 
@@ -357,6 +372,7 @@
         o_loc[ch["j"], ch["r"]] = s[:, :hd]
         r_mat[ch["j"], ch["r"]] = ch["qe"] - s[:, hd:]
 
+    pass_on(0)
     pl.when(chip > 0)(lambda: halo(0).wait_recv())
     pl.when(chip < chips - 1)(lambda: halo(1).wait_recv())
     span = rows + 2 * WINDOW
@@ -375,22 +391,38 @@
         p = e / (jnp.sum(e, axis=-1, keepdims=True) + jnp.exp(sink - m))
         heads[j, :, :hd] = plain(p.astype(BF16), kvbuf[keys, hd:]).astype(BF16)
 
-    ident = jnp.concatenate([none, e64], axis=1).astype(BF16)
-    sums, prods = [none, none], [e64, e64]
     for d in range(1, chips):
-        for r in range(2):
-            there = chip - d if r == 0 else chip + d
-            ok = there >= 0 if r == 0 else there < chips
-
-            @pl.when(ok)
-            def _(there=there):
-                copy_to(st.at[0], stbuf.at[there], st_s.at[0], st_r.at[there], (me, t)).wait_recv()
-
-            move = jnp.where(ok, stbuf[jnp.where(ok, there, chip)], ident)
-            high, low = split(prods[r])
-            step = plain(jnp.concatenate([high, low], axis=1), jnp.concatenate([move, move], axis=0))
-            sums[r] = sums[r] + step[:, :hd]
-            prods[r] = step[:, hd:]
+        there = lax.rem(chip + d, chips)
+        copy_to(st.at[0], stbuf.at[there], st_s.at[0], st_r.at[there], (me, t)).wait_recv()
+
+    def follow(late, early):
+        full = close(split(late[:, hd:]), split(early))
+        return full + jnp.concatenate([late[:, :hd], none], axis=1)
+
+    def first_follow(late, early):
+        full = plain(late[:, hd:], early)
+        return full + jnp.concatenate([late[:, :hd].astype(F32), none], axis=1)
+
+    ident = jnp.concatenate([none, e64], axis=1)
+    kin = []
+    for level in range(4):
+        size = 1 << level
+        before = lax.rem(lax.div(chip, size), 2) == 1
+        base = (lax.div(chip, size) + jnp.where(before, -1, 1)) * size
+        group = [stbuf[base + i] for i in range(size)]
+        merge = first_follow
+        while len(group) > 1:
+            group = [
+                merge(jnp.where(before, hi, lo), jnp.where(before, lo, hi))
+                for lo, hi in zip(group[::2], group[1::2])
+            ]
+            merge = follow
+        kin.append((before, group[0].astype(F32)))
+    sums = []
+    for r in range(2):
+        steps = [jnp.where(ok if r == 0 else ~ok, move, ident) for ok, move in kin]
+        near_part = follow(follow(steps[0], steps[1]), steps[2])
+        sums.append(near(near_part[:, hd:], steps[3][:, :hd]) + near_part[:, :hd])
     for j in range(2):
         o = o_loc[j, 0] + o_loc[j, 1]
         for r in range(2):
@@ -417,18 +449,17 @@
     for c in hands:
         c.start()
     gath[2 * t + core] = heads[core, spot(t)]
-    for c in tok_copies + x_copies:
+    for c in tok_copies:
         c.wait_send()
     w1.drain()
     w2.drain()
     os.drain()
-    for d in range(1, nt):
-        j = lax.rem(t + d, nt)
-        x_copy(0, j, j).wait_recv()
-        share(j, core).start()
-    for j in range(nt):
-        share(j, core).wait_send()
-        share(j, 1 - core).wait_recv()
+    for db in (1, 3, 2):
+        pass_on(db)
+    for db in range(RING):
+        x_all(db, lambda c: c.wait_send())
+        own_class(lambda c: share(db, c).wait_send())
+        own_class(lambda c: share(db, 1 - c).wait_recv())
     pl.when(chip < chips - 1)(lambda: halo(0).wait_send())
     pl.when(chip > 0)(lambda: halo(1).wait_send())
     state_all(lambda c: c.wait_send())
@@ -482,7 +513,7 @@
             vm((2, kb, 4 * hd), BF16),
             vm((n * kb, 4 * hd), BF16),
             vm((n * kb, 4 * hd), BF16),
-            vm((chips, 2, cw, nt * 4 * hd), BF16),
+            vm((RING, RING, 2, cw, nt * 4 * hd), BF16),
             vm((2 * rows, 4 * hd), F32),
             vm((2 * rows, 4 * hd), F32),
             vm((2 * rows + 2 * WINDOW, 2 * hd), BF16),
@@ -495,8 +526,8 @@
             dma((2 * nt - 1,)), dma((nt, 2)),
             dma((n - 1,)), dma((n,)),
             dma((n - 1,)), dma((n,)),
-            dma((nt - 1,)), dma((nt,)),
-            dma((nt,)), dma((nt,)),
+            dma((RING, nt - 1)), dma((RING, nt)),
+            dma((RING,)), dma((RING,)),
             dma((n - 1,)), dma((n,)),
             dma((2,)), dma((2,)),
             dma((chips,)), dma((chips,)),

time: 41.8 us -> 37.1 us (0.89)
  Pallas kernels: 41 us -> 36.3 us
    pallas_call x1, Pallas kernels: 41 us -> 36.3 us  [per_device(): pl.pallas_call(functools.partial(layer_kernel, n, nt), out_shape=jax.Shap...]
where the time goes in v4:
time: 37.1 us; the launch traced here: 36.9 us
  Pallas kernels  36.3 us (98%)
  local copies, waits for them, and re-layouts  0.63 us (2%)
    pallas_call x1, Pallas kernels, per_device(): pl.pallas_call(functools.partial(layer_kernel, n, nt), out_shape=jax.Shap...  36.3 us

profile of v4, /device:TPU:1, one launch (start us, length us, event | category | flops | bytes accessed | tf_op | source)
XLA Modules:
  0.0 36.9 jit_solution(12719803557232042797)
XLA Ops:
  0.0 36.3 %shard_map.163 = bf16[32,1024]{1,0:T(8,128)(2,1)S(1)} custom-call(bf16[128,256]{1,0:T(8,128)(2,1)} %tok_in.1, f32[1,1024]{1,0:T(1,128)} %bitcast.12, bf16[32,128]{1,0:T(8,128)(2,1)} %aq_in.1, bf16[32,64]{1,0:T(8,128)(2,1)} %ak_in.1, bf16[32,64]{1,0:T(8,128)(2,1)} %av_in.1, bf16[32,128]{1,0:T(8,128)(2,1)} %dq_in.1, bf16[32,128]{1,0:T(8,128)(2,1)} %dk_in.1, ...), custom_call_target="tpu_custom_call" | custom-call | tf_op jit(solution)/shard_map/pallas_call | solution.py:493
  36.3 0.6 %copy.19 = bf16[32,1024]{1,0:T(8,128)(2,1)} copy(bf16[32,1024]{1,0:T(8,128)(2,1)S(1)} %shard_map.163) | data formatting | bytes 131072

commit v5 on v4

--- a/solution.py
+++ b/solution.py
@@ -147,9 +147,8 @@
     for c in loads:
         c.start()
 
-    feats = lambda i: pl.ds(pl.multiple_of(i * 4 * hd, 4 * hd), 4 * hd)
     rows_of = lambda buf: lambda blk: buf.at[pl.ds(blk * kb, kb)]
-    o_rows = lambda blk: obuf.at[lax.div(blk, 2 * RING), lax.rem(lax.div(blk, 2), RING), lax.rem(blk, 2), :, feats(t)]
+    o_rows = lambda blk: obuf.at[t, lax.div(blk, 2 * RING), lax.rem(lax.div(blk, 2), RING), lax.rem(blk, 2)]
     w1 = Spread(core, z, y, t, rows_of(wbuf1), lambda c: pack1.at[c], w1_s, w1_r)
     w2 = Spread(core, z, y, t, rows_of(wbuf2), lambda c: pack2.at[c], w2_s, w2_r)
     os = Spread(core, z, y, t, o_rows, lambda c: o_rows(me), o_s, o_r, single=True)
@@ -182,7 +181,7 @@
         pack1[c], pack2[c] = packs[0][c], packs[1][c]
     wbuf1[mine] = jnp.where(core == 0, packs[0][0], packs[0][1])
     wbuf2[mine] = jnp.where(core == 0, packs[1][0], packs[1][1])
-    obuf[z, y, core, :, feats(t)] = jnp.concatenate(
+    obuf[t, z, y, core] = jnp.concatenate(
         [oin[0][:, :hd], oin[1][:, :hd], oin[0][:, hd:], oin[1][:, hd:]], axis=1
     )
     pl.semaphore_wait(bar, 12 + nt)
@@ -224,20 +223,19 @@
     for j in range(nt):
         tok_copy(0, j, 1 - core, (partner, t)).wait_recv()
     norm(1 - core)
-    w2.forward()
     os.forward()
 
     def own_class(act):
         for c in range(2):
             pl.when(core == c)(lambda c=c: act(c))
 
-    def band(db, c, cols):
+    def band(db, c, j):
         if c == 0:
-            return obuf.at[lax.rem(z + db, RING), :, 0, :, cols]
-        return obuf.at[:, lax.rem(y + db, RING), 1, :, cols]
+            return obuf.at[j, lax.rem(z + db, RING), :, 0]
+        return obuf.at[j, :, lax.rem(y + db, RING), 1]
 
     def x_copy(db, d, c, j):
-        ref = band(db, c, feats(j))
+        ref = band(db, c, j)
         return copy_to(ref, ref, x_s.at[db, d - 1], x_r.at[db, j], (me, lax.rem(t + d, nt)))
 
     def x_all(db, act):
@@ -245,7 +243,7 @@
             own_class(lambda c, d=d: act(x_copy(db, d, c, t)))
 
     def share(db, c):
-        ref = band(db, c, pl.ds(0, nt * 4 * hd))
+        ref = band(db, c, slice(None))
         return copy_to(ref, ref, g_s.at[db], g_r.at[db], (partner, t))
 
     def pass_on(db):
@@ -254,6 +252,7 @@
         own_class(lambda c: share(db, c).start())
 
     x_all(0, lambda c: c.start())
+    w2.forward()
     w1.finish()
 
     acc1[...] = plain(normed[...], wbuf1[...])
@@ -312,6 +311,9 @@
         xs = [split(x) for x in inv]
         left = [close(x, (m * a[0], m * a[1])) for x, a in zip(xs, pairs)]
         inv = [x - close(split(y_), z_) for x, y_, z_ in zip(inv, left, xs)]
+    for db in (1, 3, 2):
+        os.finish((db if db < 3 else -1,))
+        x_all(db, lambda c: c.start())
     sols = [split(close(split(x), split(ch["rhs"]))) for x, ch in zip(inv, chains)]
     outs = [close(split(ch["kd"]), s) for ch, s in zip(chains, sols)]
     e64 = jnp.where(
@@ -329,18 +331,19 @@
         full += jnp.concatenate([late[:, :hd], none], axis=1)
         st[r] = full.astype(BF16)
 
-    for db in (1, 3, 2):
-        os.finish((db if db < 3 else -1,))
-        x_all(db, lambda c: c.start())
-    def state_copy(r, p):
-        return copy_to(st.at[r], stbuf.at[chip], st_s.at[p], st_r.at[chip], (2 * p + core, t))
-
-    def state_all(act):
-        for d in range(1, chips):
-            pl.when(chip + d < chips)(lambda d=d: act(state_copy(0, chip + d)))
-            pl.when(chip - d >= 0)(lambda d=d: act(state_copy(1, chip - d)))
-
-    state_all(lambda c: c.start())
+    offsets = sorted(
+        [(dz, dy) for dz in (0, 1, -1, 2) for dy in (0, 1, -1, 2) if dz or dy], key=lambda o: -abs(o[0]) - abs(o[1])
+    )
+
+    def state_copy(k):
+        p = w1.chip(0, offsets[k][1], offsets[k][0])
+        return copy_to(
+            st.at[jnp.where(p > chip, 0, 1)], stbuf.at[chip], st_s.at[k], st_r.at[chip], (2 * p + core, t)
+        )
+
+    states = [state_copy(k) for k in range(chips - 1)]
+    for c in states:
+        c.start()
     w2.finish()
     acc2[...] = plain(normed[...], wbuf2[...])
     both = 2 * rows
@@ -369,8 +372,13 @@
     pl.when(chip > 0)(lambda: halo(1).start())
     inner = [close(split(ch["pm"]), s) for ch, s in zip(chains, sols)]
     for ch, s in zip(chains, inner):
-        o_loc[ch["j"], ch["r"]] = s[:, :hd]
-        r_mat[ch["j"], ch["r"]] = ch["qe"] - s[:, hd:]
+        j, r = ch["j"], ch["r"]
+        local, reach = s[:, :hd], ch["qe"] - s[:, hd:]
+        if j != r:
+            step = close(split(reach), split(moves[2 * (1 - j) + r]))
+            local, reach = local + step[:, :hd], step[:, hd:]
+        o_loc[j, r] = local
+        r_mat[j, r] = reach
 
     pass_on(0)
     pl.when(chip > 0)(lambda: halo(0).wait_recv())
@@ -425,12 +433,8 @@
         sums.append(near(near_part[:, hd:], steps[3][:, :hd]) + near_part[:, :hd])
     for j in range(2):
         o = o_loc[j, 0] + o_loc[j, 1]
-        for r in range(2):
-            state = sums[r]
-            if j != r:
-                prev = moves[2 * (1 - j) + r]
-                state = near(prev[:, hd:], state) + prev[:, :hd]
-            o += near(r_mat[j, r], state)
+        reach = split(jnp.concatenate([r_mat[j, 0], r_mat[j, 1]], axis=1))
+        o += close(reach, split(jnp.concatenate(sums, axis=0)))
         o = o * lax.rsqrt(jnp.mean(o * o, axis=-1, keepdims=True) + norm_eps) * og[...]
         gate = acc2[j * rows : (j + 1) * rows, hd : 2 * hd].astype(BF16).astype(F32)
         heads[j, :, hd:] = (o * silu(gate)).astype(BF16)
@@ -462,12 +466,16 @@
         own_class(lambda c: share(db, 1 - c).wait_recv())
     pl.when(chip < chips - 1)(lambda: halo(0).wait_send())
     pl.when(chip > 0)(lambda: halo(1).wait_send())
-    state_all(lambda c: c.wait_send())
+    for c in states:
+        c.wait_send()
     for x, c in peers:
         ref = gath.at[2 * x + c]
         copy_to(ref, ref, h_s.at[0], h_r.at[2 * x + c], (2 * chip + c, x)).wait_recv()
-    lhs = jnp.concatenate([gath[i] for i in range(2 * nt)], axis=1)
-    out[...] = plain(lhs, obuf[...].reshape(n * kb, -1), ((1,), (1,))).astype(BF16)
+    total = jnp.zeros(out.shape, F32)
+    for x in range(nt):
+        lhs = jnp.concatenate([gath[2 * x], gath[2 * x + 1]], axis=1)
+        total += plain(lhs, obuf[x].reshape(n * kb, -1), ((1,), (1,)))
+    out[...] = total.astype(BF16)
     for c in hands:
         c.wait_send()
 
@@ -513,7 +521,7 @@
             vm((2, kb, 4 * hd), BF16),
             vm((n * kb, 4 * hd), BF16),
             vm((n * kb, 4 * hd), BF16),
-            vm((RING, RING, 2, cw, nt * 4 * hd), BF16),
+            vm((nt, RING, RING, 2, cw, 4 * hd), BF16),
             vm((2 * rows, 4 * hd), F32),
             vm((2 * rows, 4 * hd), F32),
             vm((2 * rows + 2 * WINDOW, 2 * hd), BF16),

time: 37.1 us -> 36 us (0.970)
  Pallas kernels: 36.3 us -> 35.3 us
    pallas_call x1, Pallas kernels: 36.3 us -> 35.3 us  [per_device(): pl.pallas_call(functools.partial(layer_kernel, n, nt), out_shape=jax.Shap...]
where the time goes in v5:
time: 36 us; the launch traced here: 35.9 us
  Pallas kernels  35.3 us (98%)
  local copies, waits for them, and re-layouts  0.63 us (2%)
    pallas_call x1, Pallas kernels, per_device(): pl.pallas_call(functools.partial(layer_kernel, n, nt), out_shape=jax.Shap...  35.3 us

profile of v5, /device:TPU:1, one launch (start us, length us, event | category | flops | bytes accessed | tf_op | source)
XLA Modules:
  0.0 35.9 jit_solution(5772188171084437850)
XLA Ops:
  0.0 35.3 %shard_map.163 = bf16[32,1024]{1,0:T(8,128)(2,1)S(1)} custom-call(bf16[128,256]{1,0:T(8,128)(2,1)} %tok_in.1, f32[1,1024]{1,0:T(1,128)} %bitcast.12, bf16[32,128]{1,0:T(8,128)(2,1)} %aq_in.1, bf16[32,64]{1,0:T(8,128)(2,1)} %ak_in.1, bf16[32,64]{1,0:T(8,128)(2,1)} %av_in.1, bf16[32,128]{1,0:T(8,128)(2,1)} %dq_in.1, bf16[32,128]{1,0:T(8,128)(2,1)} %dk_in.1, ...), custom_call_target="tpu_custom_call" | custom-call | tf_op jit(solution)/shard_map/pallas_call | solution.py:501
  35.3 0.6 %copy.19 = bf16[32,1024]{1,0:T(8,128)(2,1)} copy(bf16[32,1024]{1,0:T(8,128)(2,1)S(1)} %shard_map.163) | data formatting | bytes 131072

commit v6 on v5

--- a/solution.py
+++ b/solution.py
@@ -271,7 +271,12 @@
         tail = acc1[part_rows, 2 * hd :]
         soft = jnp.maximum(tail, 0.0) + jnp.log1p(jnp.exp(-jnp.abs(tail)))
         g = coef * soft
-        cums = [exact(m, g) for m in ones]
+        hi_g = g.astype(BF16)
+        mid = (g - hi_g.astype(F32))
+        mid_g = mid.astype(BF16)
+        low_g = (mid - mid_g.astype(F32)).astype(BF16)
+        gs = jnp.concatenate([hi_g, mid_g, low_g], axis=0)
+        cums = [plain(jnp.concatenate([m.astype(BF16)] * 3, axis=1), gs) for m in ones]
         columns = jnp.where(
             lane == hd + 2, cums[0],
             jnp.where(lane == hd + 3, cums[1], jax.nn.sigmoid(tail + shift_row)),
@@ -431,6 +436,7 @@
         steps = [jnp.where(ok if r == 0 else ~ok, move, ident) for ok, move in kin]
         near_part = follow(follow(steps[0], steps[1]), steps[2])
         sums.append(near(near_part[:, hd:], steps[3][:, :hd]) + near_part[:, :hd])
+    pass_on(1)
     for j in range(2):
         o = o_loc[j, 0] + o_loc[j, 1]
         reach = split(jnp.concatenate([r_mat[j, 0], r_mat[j, 1]], axis=1))
@@ -458,7 +464,7 @@
     w1.drain()
     w2.drain()
     os.drain()
-    for db in (1, 3, 2):
+    for db in (3, 2):
         pass_on(db)
     for db in range(RING):
         x_all(db, lambda c: c.wait_send())

time: 36 us -> 36 us (level)
  no operation moved by 1% of the time
where the time goes in v6:
time: 36 us; the launch traced here: 35.8 us
  Pallas kernels  35.2 us (98%)
  local copies, waits for them, and re-layouts  0.63 us (2%)
    pallas_call x1, Pallas kernels, per_device(): pl.pallas_call(functools.partial(layer_kernel, n, nt), out_shape=jax.Shap...  35.2 us

profile of v6, /device:TPU:1, one launch (start us, length us, event | category | flops | bytes accessed | tf_op | source)
XLA Modules:
  0.0 35.8 jit_solution(16344928605228104538)
XLA Ops:
  0.0 35.2 %shard_map.163 = bf16[32,1024]{1,0:T(8,128)(2,1)S(1)} custom-call(bf16[128,256]{1,0:T(8,128)(2,1)} %tok_in.1, f32[1,1024]{1,0:T(1,128)} %bitcast.12, bf16[32,128]{1,0:T(8,128)(2,1)} %aq_in.1, bf16[32,64]{1,0:T(8,128)(2,1)} %ak_in.1, bf16[32,64]{1,0:T(8,128)(2,1)} %av_in.1, bf16[32,128]{1,0:T(8,128)(2,1)} %dq_in.1, bf16[32,128]{1,0:T(8,128)(2,1)} %dk_in.1, ...), custom_call_target="tpu_custom_call" | custom-call | tf_op jit(solution)/shard_map/pallas_call | solution.py:507
  35.2 0.6 %copy.19 = bf16[32,1024]{1,0:T(8,128)(2,1)} copy(bf16[32,1024]{1,0:T(8,128)(2,1)S(1)} %shard_map.163) | data formatting | bytes 131072

commit v7 on v6

--- a/solution.py
+++ b/solution.py
@@ -459,13 +459,13 @@
     for c in hands:
         c.start()
     gath[2 * t + core] = heads[core, spot(t)]
+    for db in (3, 2):
+        pass_on(db)
     for c in tok_copies:
         c.wait_send()
     w1.drain()
     w2.drain()
     os.drain()
-    for db in (3, 2):
-        pass_on(db)
     for db in range(RING):
         x_all(db, lambda c: c.wait_send())
         own_class(lambda c: share(db, c).wait_send())

time: 36 us -> 36 us (level)
  no operation moved by 1% of the time
where the time goes in v7:
time: 36 us; the launch traced here: 35.8 us
  Pallas kernels  35.2 us (98%)
  local copies, waits for them, and re-layouts  0.63 us (2%)
    pallas_call x1, Pallas kernels, per_device(): pl.pallas_call(functools.partial(layer_kernel, n, nt), out_shape=jax.Shap...  35.2 us

profile of v7, /device:TPU:1, one launch (start us, length us, event | category | flops | bytes accessed | tf_op | source)
XLA Modules:
  0.0 35.8 jit_solution(12359276954387667011)
XLA Ops:
  0.0 35.2 %shard_map.163 = bf16[32,1024]{1,0:T(8,128)(2,1)S(1)} custom-call(bf16[128,256]{1,0:T(8,128)(2,1)} %tok_in.1, f32[1,1024]{1,0:T(1,128)} %bitcast.12, bf16[32,128]{1,0:T(8,128)(2,1)} %aq_in.1, bf16[32,64]{1,0:T(8,128)(2,1)} %ak_in.1, bf16[32,64]{1,0:T(8,128)(2,1)} %av_in.1, bf16[32,128]{1,0:T(8,128)(2,1)} %dq_in.1, bf16[32,128]{1,0:T(8,128)(2,1)} %dk_in.1, ...), custom_call_target="tpu_custom_call" | custom-call | tf_op jit(solution)/shard_map/pallas_call | solution.py:507
  35.2 0.6 %copy.19 = bf16[32,1024]{1,0:T(8,128)(2,1)} copy(bf16[32,1024]{1,0:T(8,128)(2,1)S(1)} %shard_map.163) | data formatting | bytes 131072
